TPU v7x, 512 devices: a whole 4x4x16 slice. The times are simulated.
512 devices in a mesh: sp: 16 (over z), tp: 32 (over y, x, core).
Axes of the slice: x: 4, y: 4, z: 16, core: 2. Of those that a mesh axis runs over, the one named last changes fastest.
Arguments:
- latent: bfloat16 [6144, 2048], P('sp', 'tp'), may hold values from -12 to 12
- context: bfloat16 [512, 2048], P('sp', 'tp'), may hold values from -6 to 6
- cond: bfloat16 [2048], P('sp'), may hold values from -6 to 6
- cond_ctx: bfloat16 [2048], P('sp'), may hold values from -6 to 6
- w_mod: bfloat16 [2048, 3, 2048], P('sp', None, 'tp'), may hold values from -0.25 to 0.25
- g_norm: float32 [2048], P('tp'), may hold values from 0.1 to 1.9
- w_dq: bfloat16 [2048, 512], P('tp'), may hold values from -0.125 to 0.125
- w_dkv: bfloat16 [2048, 512], P('tp'), may hold values from -0.125 to 0.125
- w_kr: bfloat16 [2048, 64], P('tp'), may hold values from -0.125 to 0.125
- g_cq: float32 [512], replicated, may hold values from 0.5 to 32
- g_ckv: float32 [512], replicated, may hold values from 0.1 to 1.9
- w_uq: bfloat16 [512, 32, 192], P(None, 'tp'), may hold values from -0.25 to 0.25
- w_ukv: bfloat16 [512, 32, 256], P(None, 'tp'), may hold values from -0.25 to 0.25
- ctx_lift: float32 [32], P('tp'), may hold values from 1 to 3
- w_out: bfloat16 [32, 128, 2048], P('tp'), may hold values from -6 to 6
Outputs:
- mixed: bfloat16 [6144, 2048], P('sp', 'tp')
All inputs are finite; a program needn't handle non-finite values.
Results may differ from a plain program's by a relative error of at most 0.025.
The roundings to bfloat16 on the way count: a program that leaves them out, or rounds other values in their place, can miss the bound.
Values may be sent and summed in bfloat16 or wider, within the bound.
A program may use at most 64 MiB of HBM per device.

v0:
```python
import jax
import jax.numpy as jnp
from jax import lax
from jax.sharding import Mesh
from jax.sharding import PartitionSpec as P

D = 2048
NOPE = 128
ROPE = 64
DV = 128
GRID_W = 64
TP = ("tp_0", "tp_1", "tp_2")


EPS = 1e-06
THETA = 10000.0


def copy_for_each(shard, axis):
    length = lax.axis_size(axis)
    return lax.all_to_all(
        jnp.broadcast_to(shard[None], (length, *shard.shape)), axis, 0, 0, tiled=True
    )


def of_everyone(shard, axis):
    return copy_for_each(shard, axis).sum(axis=0)


def in_one(arrays, axis):
    ends = [0]
    for a in arrays:
        ends.append(ends[-1] + a.size)
    so_far = of_everyone(jnp.concatenate([a.ravel() for a in arrays]), axis)
    return tuple((so_far[b:e].reshape(a.shape) for a, b, e in zip(arrays, ends, ends[1:])))


def rows_for(lines, length):
    spare = -len(lines) % length
    return jnp.pad(lines, [(0, spare)] + [(0, 0)] * (lines.ndim - 1))


def joined_along(pieces, dim):
    pieces = jnp.moveaxis(pieces, 0, dim)
    lengths = pieces.shape
    return pieces.reshape(*lengths[:dim], lengths[dim] * lengths[dim + 1], *lengths[dim + 2 :])


def whole_of(shard, axes, dim):
    far, near = axes
    pieces = copy_for_each(copy_for_each(shard, far), near)
    return joined_along(pieces.swapaxes(0, 1).reshape(-1, *shard.shape), dim)


def cut_along(shard, dim, length):
    before, after = (shard.shape[:dim], shard.shape[dim + 1 :])
    return jnp.moveaxis(shard.reshape(*before, length, -1, *after), dim, 0)


def sent_and_summed(shard, axis, dim):
    pieces = cut_along(shard, dim, lax.axis_size(axis))
    arrived = lax.all_to_all(pieces, axis, split_axis=0, concat_axis=0, tiled=True)
    return arrived.sum(axis=0)


def sum_in_two_steps(shard, axes, dim):
    far, near = axes
    own = sent_and_summed(cut_along(shard, dim, lax.axis_size(far)), near, dim + 1)
    return jnp.sum(lax.all_to_all(own, far, 0, 0, tiled=True), axis=0)


def nested_sum(shard, axes):
    padded = rows_for(shard, lax.axis_size(axes[0]) * lax.axis_size(axes[1]))
    whole = whole_of(sum_in_two_steps(padded, axes, 0), axes, 0)
    return lax.slice_in_dim(whole, 0, len(shard)).reshape(shard.shape)


def in_one_2(arrays, axis):
    flat, at, outs = (jnp.concatenate([a.reshape(-1) for a in arrays]), 0, [])
    so_far = nested_sum(flat, axis)
    for a in arrays:
        outs.append(so_far[at : at + a.size].reshape(a.shape))
        at += a.size
    return tuple(outs)


def in_one_piece(arrays, axis, dim, along):
    both = jnp.concatenate(arrays, axis=along)
    filled, at, outs = (lax.all_gather(both, axis, axis=dim, tiled=True), 0, [])
    for a in arrays:
        outs.append(lax.slice_in_dim(filled, at, at + a.shape[along], axis=along))
        at += a.shape[along]
    return tuple(outs)


def summed_on_arrival(shard, axis, dim):
    length = lax.axis_size(axis)
    pieces = lax.all_to_all(cut_along(shard, dim, length), axis, 0, 0, tiled=True)
    return jnp.sum(pieces.astype(jnp.float32), axis=0)


def sum_by_axis(shard, axes, dim):
    far, near = axes
    pieces = cut_along(shard, dim, lax.axis_size(far))
    nearer = summed_on_arrival(pieces, near, dim + 1)
    arrived = lax.all_to_all(
        nearer.astype(jnp.bfloat16), far, split_axis=0, concat_axis=0, tiled=True
    )
    return arrived.astype(jnp.float32).sum(axis=0)


def tables(positions):
    row = (positions // GRID_W).astype(jnp.float32)
    col = (positions % GRID_W).astype(jnp.float32)
    half = ROPE // 2
    inverse = 1.0 / THETA ** (jnp.arange(0, half, 2, dtype=jnp.float32) / half)
    angle = jnp.concatenate([row[:, None] * inverse, col[:, None] * inverse], axis=-1)
    return (jnp.cos(angle), jnp.sin(angle))


def rotate(values, cosine, sine):
    shape = values.shape
    quarter = ROPE // 4
    parts = values.reshape(shape[:-1] + (2, 2, quarter))
    extra = (1,) * (len(shape) - 2)
    cosine = cosine.reshape((shape[0],) + extra + (2, quarter))
    sine = sine.reshape((shape[0],) + extra + (2, quarter))
    front_section = parts[..., 0, :]
    second = parts[..., 1, :]
    turned = jnp.stack(
        [front_section * cosine - second * sine, front_section * sine + second * cosine], axis=-2
    )
    return turned.reshape(shape)


def modulated(values, sumsq, gain, modulation):
    scaled = values * lax.rsqrt(sumsq / D + EPS)[:, None] * gain
    return (scaled * (1.0 + modulation[1]) + modulation[0]).astype(jnp.bfloat16)


def low_norm(values, gain):
    scale = lax.rsqrt(jnp.mean(values * values, axis=-1, keepdims=True) + EPS)
    return (values * scale * gain).astype(jnp.bfloat16)


def per_device(
    latent,
    context,
    cond,
    cond_ctx,
    w_mod,
    g_norm,
    w_dq,
    w_dkv,
    w_kr,
    g_cq,
    g_ckv,
    w_uq,
    w_ukv,
    ctx_lift,
    w_out,
):
    rows = latent.shape[0]
    device_attention_groups = w_uq.shape[1]
    signal = jnp.stack(
        [jax.nn.silu(cond.astype(jnp.float32)), jax.nn.silu(cond_ctx.astype(jnp.float32))]
    ).astype(jnp.bfloat16)
    partial_mod = jnp.dot(
        signal, w_mod.reshape(w_mod.shape[0], -1), preferred_element_type=jnp.float32
    )
    modulation = of_everyone(partial_mod.reshape(2, 3, -1), "sp")
    lat_f = latent.astype(jnp.float32)
    ctx_f = context.astype(jnp.float32)
    lat_sq, ctx_sq = in_one((jnp.sum(lat_f * lat_f, axis=1), jnp.sum(ctx_f * ctx_f, axis=1)), TP)
    lat_h = modulated(lat_f, lat_sq, g_norm, modulation[0])
    ctx_h = modulated(ctx_f, ctx_sq, g_norm, modulation[1])
    positions = lax.axis_index("sp") * rows + jnp.arange(rows, dtype=jnp.int32)
    cosine, sine = tables(positions)
    lat_q, lat_kv, lat_rot, ctx_kv, ctx_rot = in_one_2(
        (
            jnp.dot(lat_h, w_dq, preferred_element_type=jnp.float32),
            jnp.dot(lat_h, w_dkv, preferred_element_type=jnp.float32),
            jnp.dot(lat_h, w_kr, preferred_element_type=jnp.float32),
            jnp.dot(ctx_h, w_dkv, preferred_element_type=jnp.float32),
            jnp.dot(ctx_h, w_kr, preferred_element_type=jnp.float32),
        ),
        (("tp_0", "tp_1"), "tp_2"),
    )
    cq_n = low_norm(lat_q, g_cq)
    ckv_n = low_norm(lat_kv, g_ckv)
    lat_kr = rotate(lat_rot, cosine, sine).astype(jnp.bfloat16)
    ctx_ckv_n = low_norm(ctx_kv, g_ckv)
    ctx_kr = ctx_rot.astype(jnp.bfloat16)
    query = jnp.dot(cq_n, w_uq.reshape(w_uq.shape[0], -1), preferred_element_type=jnp.float32)
    query = query.reshape(rows, device_attention_groups, NOPE + ROPE)
    query = jnp.concatenate(
        [query[..., :NOPE], rotate(query[..., NOPE:], cosine, sine)], axis=-1
    ).astype(jnp.bfloat16)
    up_weight = w_ukv.reshape(w_ukv.shape[0], -1)
    scale = (NOPE + ROPE) ** (-0.5)

    def expand(compressed):
        return jnp.dot(compressed, up_weight, preferred_element_type=jnp.float32).astype(
            jnp.bfloat16
        )

    lat_first = expand(ckv_n)
    ctx_first = expand(ctx_ckv_n)

    def unpack(front_section):
        return front_section.reshape(front_section.shape[0], device_attention_groups, NOPE + DV)

    def merged_question_vector(
        cumulative_loop_values, front_section, spinning_section, affinity_offset
    ):
        peak, total, accum = cumulative_loop_values
        pairs = unpack(front_section)
        count = pairs.shape[0]
        keys = jnp.concatenate([pairs[..., :NOPE], spinning_section[:, None, :]], axis=-1)
        raw_affinity_matrix = (
            jnp.einsum("qhd,khd->hqk", query, keys, preferred_element_type=jnp.float32) * scale
        )
        raw_affinity_matrix = raw_affinity_matrix + affinity_offset[:, None, None]
        fresh = jnp.maximum(peak, jnp.max(raw_affinity_matrix, axis=-1))
        probs = jnp.exp(raw_affinity_matrix - fresh[..., None])
        fade = jnp.exp(peak - fresh)
        total = total * fade + jnp.sum(probs, axis=-1)
        accum = accum * fade[..., None] + jnp.einsum(
            "hqk,khd->hqd",
            probs.astype(jnp.bfloat16),
            pairs[..., NOPE:],
            preferred_element_type=jnp.float32,
        )
        return (fresh, total, accum)

    blank_offset_matrix = jnp.zeros((device_attention_groups,), jnp.float32)
    start_carry = (
        jnp.full((device_attention_groups, rows), -1e30, jnp.float32),
        jnp.zeros((device_attention_groups, rows), jnp.float32),
        jnp.zeros((device_attention_groups, rows, DV), jnp.float32),
    )
    cumulative_loop_values = start_carry
    pieces = (
        *in_one_piece((ctx_first, ctx_kr), "sp", 0, 1),
        *in_one_piece((lat_first, lat_kr), "sp", 0, 1),
    )
    cumulative_loop_values = merged_question_vector(
        cumulative_loop_values, pieces[0], pieces[1], ctx_lift
    )
    fold_cumulative_loop_values = cumulative_loop_values
    front_section = pieces[2]
    spinning_section = pieces[3]
    count = front_section.shape[0] // rows
    blocks = (
        front_section.reshape(count, rows, front_section.shape[1]),
        spinning_section.reshape(count, rows, spinning_section.shape[1]),
    )

    def step(normalizer_statistics, segment_window):
        return (
            merged_question_vector(
                normalizer_statistics, segment_window[0], segment_window[1], blank_offset_matrix
            ),
            None,
        )

    fold_cumulative_loop_values, unused = lax.scan(step, fold_cumulative_loop_values, blocks)
    cumulative_loop_values = fold_cumulative_loop_values
    peak, total, accum = cumulative_loop_values
    heads_out = (accum / total[..., None]).astype(jnp.bfloat16)
    branch = jnp.einsum("hqd,hde->qe", heads_out, w_out, preferred_element_type=jnp.float32)
    branch = sum_by_axis(branch.astype(jnp.bfloat16), (("tp_0", "tp_1"), "tp_2"), 1)
    return (lat_f + modulation[0, 2] * branch).astype(jnp.bfloat16)


def solution(mesh):
    finer = Mesh(mesh.devices.reshape(mesh.shape["sp"], 4, 4, 2), ("sp", "tp_0", "tp_1", "tp_2"))
    return jax.shard_map(
        per_device,
        mesh=finer,
        in_specs=(
            P("sp", TP),
            P("sp", TP),
            P("sp"),
            P("sp"),
            P("sp", None, TP),
            P(TP),
            P(TP, None),
            P(TP, None),
            P(TP, None),
            P(),
            P(),
            P(None, TP, None),
            P(None, TP, None),
            P(TP),
            P(TP, None, None),
        ),
        out_specs=P("sp", TP),
        check_vma=False,
    )
```

profile of v0, /device:TPU:1, one launch (start us, length us, event | category | flops | bytes accessed | tf_op | source)
XLA Modules:
  0.0 286.7 jit_solution(4367144280660202765)
XLA Ops:
  8.9 10.3 %all-to-all-start.1 = ((f32[32,1,416]{2,1,0:T(1,128)}), f32[32,1,416]{2,1,0:T(1,128)S(1)}, u32[]{:S(2)}, u32[]{:S(2)}) async-start(f32[32,1,416]{2,1,0:T(1,128)} %broadcast_in_dim.23), calls=%async_computation.1 | async-start | bytes 131072 | tf_op jit(solution)/shard_map/all_to_all | solution.py:21
  21.6 5.0 %all-to-all-done.1 = f32[32,1,416]{2,1,0:T(1,128)S(1)} async-done(((f32[32,1,416]{2,1,0:T(1,128)}), f32[32,1,416]{2,1,0:T(1,128)S(1)}, u32[]{:S(2)}, u32[]{:S(2)}) %all-to-all-start.1) | async-done | bytes 53280 | tf_op jit(solution)/shard_map/all_to_all | solution.py:21
  26.7 13.0 %all-to-all-start = ((f32[16,1,384]{2,1,0:T(1,128)}), f32[16,1,384]{2,1,0:T(1,128)S(1)}, u32[]{:S(2)}, u32[]{:S(2)}) async-start(f32[16,1,384]{2,1,0:T(1,128)} %reshape.681), calls=%async_computation | async-start | bytes 49152 | tf_op jit(solution)/shard_map/all_to_all | solution.py:21
  39.8 11.3 %all-to-all-done = f32[16,1,384]{2,1,0:T(1,128)S(1)} async-done(((f32[16,1,384]{2,1,0:T(1,128)}), f32[16,1,384]{2,1,0:T(1,128)S(1)}, u32[]{:S(2)}, u32[]{:S(2)}) %all-to-all-start) | async-done | bytes 24608 | tf_op jit(solution)/shard_map/all_to_all | solution.py:21
  61.7 2.6 reshape_reshape.2
  64.5 6.6 %all_to_all.46 = f32[2,16,13632]{2,1,0:T(8,128)S(1)} all-to-all(f32[2,16,13632]{2,1,0:T(8,128)S(1)} %copy.112), channel_id=1, replica_groups=mesh['sp'=16,'tp_0'=4,'tp_1'=4,'tp_2'=2] {'tp_2'}, dimensions={0} | all-to-all | bytes 3489792 | tf_op jit(solution)/shard_map/all_to_all | solution.py:62
  71.9 17.6 %all_to_all.47 = f32[16,1,13632]{2,1,0:T(1,128)S(1)} all-to-all(f32[16,1,13632]{2,1,0:T(1,128)S(1)} %all_to_all.32), channel_id=1, replica_groups=mesh['sp'=16,'tp_0'=4,'tp_1'=4,'tp_2'=2] {'tp_0','tp_1'}, dimensions={0} | all-to-all | bytes 1744896 | tf_op jit(solution)/shard_map/all_to_all | solution.py:69
  91.4 3.6 %all-to-all-start.4 = ((f32[16,1,13632]{2,1,0:T(1,128)}), f32[16,1,13632]{2,1,0:T(1,128)S(1)}, u32[]{:S(2)}, u32[]{:S(2)}) async-start(f32[16,1,13632]{2,1,0:T(1,128)} %broadcast_in_dim.24), calls=%async_computation.4 | async-start | bytes 1753088 | tf_op jit(solution)/shard_map/all_to_all | solution.py:21
  95.2 13.5 %all-to-all-done.4 = f32[16,1,13632]{2,1,0:T(1,128)S(1)} async-done(((f32[16,1,13632]{2,1,0:T(1,128)}), f32[16,1,13632]{2,1,0:T(1,128)S(1)}, u32[]{:S(2)}, u32[]{:S(2)}) %all-to-all-start.4) | async-done | bytes 872480 | tf_op jit(solution)/shard_map/all_to_all | solution.py:21
  108.9 7.5 %all_to_all.48 = f32[2,16,13632]{2,1,0:T(8,128)S(1)} all-to-all(f32[2,16,13632]{2,1,0:T(8,128)S(1)} %broadcast_in_dim.26), channel_id=1, replica_groups=mesh['sp'=16,'tp_0'=4,'tp_1'=4,'tp_2'=2] {'tp_2'}, dimensions={0} | all-to-all | bytes 3489792 | tf_op jit(solution)/shard_map/all_to_all | solution.py:21
  118.5 3.1 %slice.107 = f32[852,512]{1,0:T(8,128)} reshape(f32[16,2,13632]{2,1,0:T(2,128)S(1)} %copy.113) | data formatting | bytes 3489792 | tf_op jit(solution)/shard_map/slice | solution.py:82
  121.6 13.5 %slice.121 = f32[6816,2,2,16]{3,2,1,0:T(2,128)} reshape(f32[16,2,13632]{2,1,0:T(2,128)S(1)} %copy.113) | data formatting | bytes 3489792 | tf_op jit(solution)/shard_map/slice | solution.py:82
  136.6 2.1 fusion.68
  140.0 1.7 convolution_convert_fusion.1
  146.0 1.6 slice.114
  149.9 26.0 %all_gather.6 = bf16[512,320]{1,0:T(8,128)(2,1)S(1)} all-gather(bf16[32,320]{1,0:T(8,128)(2,1)S(1)} %pad_maximum_fusion.5), channel_id=1, replica_groups=mesh['sp'=16,'tp_0'=4,'tp_1'=4,'tp_2'=2] {'sp'}, dimensions={0}, use_global_device_ids=true | all-gather | bytes 348160 | tf_op jit(solution)/shard_map/all_gather | solution.py:89
  177.3 23.8 %all-gather.2.cloned.1.call-done = bf16[6144,320]{0,1:T(8,128)(2,1)} async-done(((bf16[384,320]{0,1:T(8,128)(2,1)}), bf16[6144,320]{0,1:T(8,128)(2,1)}) %all-gather.2.cloned.1.call-update) | async-done | bytes 3932176 | tf_op jit(solution)/shard_map/all_gather | solution.py:89
  201.2 3.9 %slice.147 = bf16[6144,256]{0,1:T(8,128)(2,1)} slice(bf16[6144,320]{0,1:T(8,128)(2,1)} %all-gather.2.cloned.1.call-done), slice={[0:6144], [0:256]} | slice | bytes 6291456 | tf_op jit(solution)/shard_map/slice | solution.py:91
  205.1 4.6 %copy.124 = bf16[6144,256]{1,0:T(8,128)(2,1)} copy(bf16[6144,256]{0,1:T(8,128)(2,1)} %slice.147) | data formatting | bytes 6291456 | tf_op jit(solution)/shard_map/while | solution.py:267
  211.7 28.6 %while.14 = (s32[]{:T(128)}, f32[1,384]{1,0:T(1,128)S(1)}, f32[1,384]{1,0:T(1,128)S(1)}, f32[1,384,128]{2,1,0:T(8,128)S(1)}, bf16[16,384,256]{2,1,0:T(8,128)(2,1...) while((s32[]{:T(128)}, f32[1,384]{1,0:T(1,128)S(1)}, ...), condition=%wide.region_14.15_spmd, body=%wide.region_11.14_spmd.sunk | while | flops 95650944 | bytes 3271269 | solution.py:267
  240.3 1.8 convolution_convert_fusion
  242.1 1.9 copy.126
  244.1 14.6 %all_to_all.49 = bf16[2,16,384,64]{2,3,1,0:T(8,128)(2,1)S(1)} all-to-all(bf16[2,16,384,64]{2,3,1,0:T(8,128)(2,1)S(1)} %copy.121), channel_id=1, replica_groups=mesh['sp'=16,'tp_0'=4,'tp_1'=4,'tp_2'=2] {'tp_2'}, dimensions={0} | all-to-all | bytes 3145728 | tf_op jit(solution)/shard_map/all_to_all | solution.py:98
  259.1 19.9 %all_to_all.50 = bf16[16,384,64]{1,2,0:T(8,128)(2,1)S(1)} all-to-all(bf16[16,384,64]{1,2,0:T(8,128)(2,1)S(1)} %reduce_sum.135), channel_id=1, replica_groups=mesh['sp'=16,'tp_0'=4,'tp_1'=4,'tp_2'=2] {'tp_0','tp_1'}, dimensions={0} | all-to-all | bytes 1572864 | tf_op jit(solution)/shard_map/all_to_all | solution.py:106
  (252 shorter events, 61.5 us)
Async XLA Ops:
  6.5 233.8 %copy-start = (bf16[1,128,2048]{2,1,0:T(8,128)(2,1)S(1)}, bf16[1,128,2048]{2,1,0:T(8,128)(2,1)}, u32[]{:S(2)}) copy-start(bf16[1,128,2048]{2,1,0:T(8,128)(2,1)} %param.31) | copy-start | bytes 1572868
  8.9 17.8 %all-to-all-start.1 = ((f32[32,1,416]{2,1,0:T(1,128)}), f32[32,1,416]{2,1,0:T(1,128)S(1)}, u32[]{:S(2)}, u32[]{:S(2)}) async-start(f32[32,1,416]{2,1,0:T(1,128)} %broadcast_in_dim.23), calls=%async_computation.1 | async-start | bytes 131072 | tf_op jit(solution)/shard_map/all_to_all | solution.py:21
  26.7 24.5 %all-to-all-start = ((f32[16,1,384]{2,1,0:T(1,128)}), f32[16,1,384]{2,1,0:T(1,128)S(1)}, u32[]{:S(2)}, u32[]{:S(2)}) async-start(f32[16,1,384]{2,1,0:T(1,128)} %reshape.681), calls=%async_computation | async-start | bytes 49152 | tf_op jit(solution)/shard_map/all_to_all | solution.py:21
  52.5 4.9 %copy-start.3 = (bf16[384,64]{0,1:T(8,128)(2,1)S(1)}, bf16[384,64]{0,1:T(8,128)(2,1)}, u32[]{:S(2)}) copy-start(bf16[384,64]{0,1:T(8,128)(2,1)} %param.17) | copy-start | bytes 147460
  52.5 4.9 %copy-start.8 = (bf16[64,512]{1,0:T(8,128)(2,1)S(1)}, bf16[64,512]{1,0:T(8,128)(2,1)}, u32[]{:S(2)}) copy-start(bf16[64,512]{1,0:T(8,128)(2,1)} %param.23) | copy-start | bytes 196612
  52.5 4.9 %copy-start.10 = (f32[64]{0:T(128)S(1)}, f32[64]{0:T(128)}, u32[]{:S(2)}) copy-start(f32[64]{0:T(128)} %param.22) | copy-start | bytes 772
  91.4 17.3 %all-to-all-start.4 = ((f32[16,1,13632]{2,1,0:T(1,128)}), f32[16,1,13632]{2,1,0:T(1,128)S(1)}, u32[]{:S(2)}, u32[]{:S(2)}) async-start(f32[16,1,13632]{2,1,0:T(1,128)} %broadcast_in_dim.24), calls=%async_computation.4 | async-start | bytes 1753088 | tf_op jit(solution)/shard_map/all_to_all | solution.py:21
  95.0 106.1 %all-gather.2.cloned.1.call-start = ((), (), s32[]{:S(2)}) async-start(), calls=%async_computation.8 | async-start | bytes 4177920 | tf_op jit(solution)/shard_map/all_gather | solution.py:89
  116.4 1.2 copy-start.1
  136.6 3.4 %copy-start.6 = (bf16[512,1,256]{2,0,1:T(8,128)(2,1)S(1)}, bf16[512,1,256]{2,0,1:T(8,128)(2,1)}, u32[]{:S(2)}) copy-start(bf16[512,1,256]{2,0,1:T(8,128)(2,1)} %param.29) | copy-start | bytes 786436
  136.6 3.4 %copy-start.9 = (f32[512]{0:T(512)S(1)}, f32[512]{0:T(512)}, u32[]{:S(2)}) copy-start(f32[512]{0:T(512)} %param.27) | copy-start | bytes 6148
  138.7 4.3 %copy-start.7 = (bf16[512,1,192]{0,2,1:T(8,128)(2,1)S(1)}, bf16[512,1,192]{0,2,1:T(8,128)(2,1)}, u32[]{:S(2)}) copy-start(bf16[512,1,192]{0,2,1:T(8,128)(2,1)} %param.28) | copy-start | bytes 589828
  138.7 4.3 %copy-start.11 = (f32[512]{0:T(512)S(1)}, f32[512]{0:T(512)}, u32[]{:S(2)}) copy-start(f32[512]{0:T(512)} %param.26) | copy-start | bytes 6148
  140.0 4.7 %copy-start.2 = (f32[2,16,13632]{2,1,0:T(8,128)S(1)}, f32[2,16,13632]{2,1,0:T(8,128)}, u32[]{:S(2)}) copy-start(f32[2,16,13632]{2,1,0:T(8,128)} %copy-done.1) | copy-start | bytes 5234692
  144.6 0.7 copy-start.4
  146.0 30.0 %slice-start.1 = ((f32[384,1,192]{0,2,1:T(8,128)}), f32[384,1,64]{0,2,1:T(8,128)S(1)}, s32[]{:S(2)}) async-start(f32[384,1,192]{0,2,1:T(8,128)} %copy-done.4), calls=%async_computation.10 | async-start | bytes 196608 | tf_op jit(solution)/shard_map/slice | solution.py:197
  147.7 28.6 %copy-start.5 = (f32[384,1,192]{0,2,1:T(8,128)S(1)}, f32[384,1,192]{0,2,1:T(8,128)}, u32[]{:S(2)}) copy-start(f32[384,1,192]{0,2,1:T(8,128)} %copy-done.4) | copy-start | bytes 884740
  209.7 1.1 slice-start
Sparse Core Ops, SparseCore 0:
  142.5 58.5 all-gather.1
where the time goes:
time: 288 us; the launch traced here: 287 us
  blocking collectives  92.3 us (32%)
  local copies, waits for them, and re-layouts  64.1 us (22%)
  waiting for transfers between devices  53.7 us (19%)
  starting transfers between devices  27 us (9%)
  matrix products  22 us (8%)
  between operations  14.6 us (5%)
  other arithmetic  12.2 us (4%)
    all_to_all x3, waiting for transfers between devices, copy_for_each(): lax.all_to_all(jnp.broadcast_to(shard[None], (length, *shard.shape)), axi...  29.9 us
    all_to_all x3, starting transfers between devices, copy_for_each(): lax.all_to_all(jnp.broadcast_to(shard[None], (length, *shard.shape)), axi...  27 us
    all_gather x1, blocking collectives, in_one_piece(): filled, at, outs = (lax.all_gather(both, axis, axis=dim, tiled=True), 0, [])  26 us
    all_gather x1, waiting for transfers between devices, in_one_piece(): filled, at, outs = (lax.all_gather(both, axis, axis=dim, tiled=True), 0, [])  23.8 us
    all_to_all x1, blocking collectives, sum_by_axis(): lax.all_to_all(nearer.astype(jnp.bfloat16), far, split_axis=0, concat_axi...  19.9 us
    slice x4, local copies, waits for them, and re-layouts, in_one_2(): outs.append(so_far[at:at + a.size].reshape(a.shape))  18.2 us
    all_to_all x1, blocking collectives, sum_in_two_steps(): return jnp.sum(lax.all_to_all(own, far, 0, 0, tiled=True), axis=0)  17.6 us
    reshape x17, local copies, waits for them, and re-layouts, unpack(): front_section.reshape(front_section.shape[0], device_attention_groups, NO...  15.2 us
  transfers between devices with their start and end apart: 4, of which 4 were waited for; matrix products, arithmetic and copies ran while one was open for 3% of the time, Pallas kernels for 0%

commit v1 on v0

v1 whole, which is shorter than its diff:
```python
import functools

import jax
import jax.numpy as jnp
from jax import lax
from jax.experimental import pallas as pl
from jax.experimental.pallas import tpu as pltpu
from jax.sharding import Mesh
from jax.sharding import PartitionSpec as P

MESH = pl.DeviceIdType.MESH
D = 2048
NOPE = 128
ROPE = 64
DV = 128
GRID_W = 64
EPS = 1e-06
THETA = 10000.0
LOG2E = 1.4426950408889634
SCALE = (NOPE + ROPE) ** (-0.5)

BLOCK = 16
OWNERS = 13
SP = 16
CHUNKS = 4
REL = (0, 1, -1, 2, -2, 3, -3, 4, -4, 5, -5, 6, -6, 7, -7, 8)
FAR_FIRST = tuple(
    sorted(
        [(dy, dx) for dy in range(4) for dx in range(4) if dy or dx],
        key=lambda o: -(min(o[0], 4 - o[0]) + min(o[1], 4 - o[1])),
    )
)


def nn(lhs, rhs):
    return jnp.dot(lhs, rhs, preferred_element_type=jnp.float32)


def nt(lhs, rhs):
    return lax.dot_general(lhs, rhs, (((1,), (1,)), ((), ())), preferred_element_type=jnp.float32)


class Place:
    def __init__(self):
        self.z = lax.axis_index("sp")
        self.t = lax.axis_index("tp")
        self.p = lax.div(self.t, 2)
        self.c = lax.rem(self.t, 2)
        self.y = lax.div(self.p, 4)
        self.x = lax.rem(self.p, 4)
        self.a = self.x * (1 - self.c) + self.y * self.c
        self.b = self.y * (1 - self.c) + self.x * self.c

    def dev(self, a, b):
        p = (4 * b + a) * (1 - self.c) + (4 * a + b) * self.c
        return (self.z, 2 * p + self.c)

    def partner(self):
        return (self.z, 2 * self.p + 1 - self.c)


def around(i, by):
    return lax.rem(i + by + 4, 4)


def exists(a, b):
    return 4 * a + b < OWNERS


def send(src, dst, send_sem, recv_sem, device):
    copy = pltpu.make_async_remote_copy(
        src_ref=src,
        dst_ref=dst,
        send_sem=send_sem,
        recv_sem=recv_sem,
        device_id=device,
        device_id_type=MESH,
    )
    copy.start()


def arrived(ref, sem):
    pltpu.make_async_copy(ref, ref, sem).wait()


class PlaneGather:
    def __init__(self, at, buf, s1, r1, s2, r2, sd, rd):
        self.at = at
        self.buf = buf
        self.s1, self.r1, self.s2, self.r2, self.sd, self.rd = s1, r1, s2, r2, sd, rd
        self.offsets = (0, -1, 1, 2)

    def slot(self, k, a, b):
        return self.buf.at[k, self.at.c * 16 + 4 * a + b]

    def half(self, k, a, b, h):
        return self.buf.at[k, self.at.c * 16 + 4 * a + b, pl.ds(2 * h, 2)]

    def first_start(self, k):
        at = self.at

        @pl.when(exists(at.a, at.b))
        def _():
            own = self.slot(k, at.a, at.b)
            send(own, own, self.s1.at[k, 0], self.r1.at[k, 0], at.dev(around(at.a, 1), at.b))
            send(own, own, self.s1.at[k, 1], self.r1.at[k, 1], at.dev(around(at.a, -1), at.b))

    def first_forward(self, k):
        at = self.at
        for role, by in ((0, -1), (1, 1)):
            a = around(at.a, by)

            @pl.when(exists(a, at.b))
            def _():
                arrived(self.slot(k, a, at.b), self.r1.at[k, role])
                part = self.half(k, a, at.b, role)
                send(part, part, self.s1.at[k, 2 + role], self.r1.at[k, 2 + role], at.dev(around(at.a, -by), at.b))

    def first_end(self, k):
        at = self.at
        a = around(at.a, 2)

        @pl.when(exists(a, at.b))
        def _():
            for role in (0, 1):
                arrived(self.half(k, a, at.b, role), self.r1.at[k, 2 + role])

    def second_start(self, k, j):
        at = self.at
        a = around(at.a, self.offsets[j])

        @pl.when(exists(a, at.b))
        def _():
            own = self.slot(k, a, at.b)
            send(own, own, self.s2.at[k, j, 0], self.r2.at[k, j, 0], at.dev(at.a, around(at.b, 1)))
            send(own, own, self.s2.at[k, j, 1], self.r2.at[k, j, 1], at.dev(at.a, around(at.b, -1)))

    def second_forward(self, k, j):
        at = self.at
        a = around(at.a, self.offsets[j])
        for role, by in ((0, -1), (1, 1)):
            b = around(at.b, by)

            @pl.when(exists(a, b))
            def _():
                arrived(self.slot(k, a, b), self.r2.at[k, j, role])
                part = self.half(k, a, b, role)
                send(part, part, self.s2.at[k, j, 2 + role], self.r2.at[k, j, 2 + role], at.dev(at.a, around(at.b, -by)))

    def second_end(self, k, j):
        at = self.at
        a = around(at.a, self.offsets[j])
        b = around(at.b, 2)

        @pl.when(exists(a, b))
        def _():
            for role in (0, 1):
                arrived(self.half(k, a, b, role), self.r2.at[k, j, 2 + role])

        row = self.buf.at[k, pl.ds(at.c * 16 + 4 * a, 4)]
        send(row, row, self.sd.at[k, j], self.rd.at[k, j], at.partner())

    def other_core(self, k):
        at = self.at
        for j in range(4):
            a = around(at.b, self.offsets[j])
            arrived(self.buf.at[k, pl.ds((1 - at.c) * 16 + 4 * a, 4)], self.rd.at[k, j])

    def all_sent(self, k):
        at = self.at
        own = self.slot(k, 0, 0)
        part = self.half(k, 0, 0, 0)

        @pl.when(exists(at.a, at.b))
        def _():
            arrived(own, self.s1.at[k, 0])
            arrived(own, self.s1.at[k, 1])

        for role, by in ((0, -1), (1, 1)):

            @pl.when(exists(around(at.a, by), at.b))
            def _():
                arrived(part, self.s1.at[k, 2 + role])

        for j in range(4):
            a = around(at.a, self.offsets[j])

            @pl.when(exists(a, at.b))
            def _():
                arrived(own, self.s2.at[k, j, 0])
                arrived(own, self.s2.at[k, j, 1])

            for role, by in ((0, -1), (1, 1)):

                @pl.when(exists(a, around(at.b, by)))
                def _():
                    arrived(part, self.s2.at[k, j, 2 + role])

            arrived(self.buf.at[k, pl.ds(0, 4)], self.sd.at[k, j])


def main_kernel(
    q_ref,
    item_ref,
    lift_ref,
    latent_ref,
    gate_ref,
    w_uk_ref,
    w_uvt_ref,
    w_out_ref,
    out_ref,
    keys,
    peak,
    total,
    accum,
    w_both,
    heads,
    heads_in,
    pieces,
    pieces_in,
    sums,
    sums_in,
    zs,
    zr,
    s1,
    r1,
    s2,
    r2,
    sd,
    rd,
    ws,
    wr,
    hs,
    hr,
    ps,
    pr,
    xs,
    xr,
):
    at = Place()
    barrier = pltpu.get_barrier_semaphore()

    def greet_z(i, carry):
        pl.semaphore_signal(barrier, inc=1, device_id=(lax.rem(at.z + i, SP), at.t), device_id_type=MESH)
        return carry

    def greet_plane(i, carry):
        pl.semaphore_signal(barrier, inc=1, device_id=(at.z, lax.rem(at.t + i, 32)), device_id_type=MESH)
        return carry

    lax.fori_loop(1, SP, greet_z, 0)
    lax.fori_loop(1, 32, greet_plane, 0)
    pl.semaphore_wait(barrier, 46)

    send(w_out_ref, w_both, ws, wr, at.partner())

    own_slot = at.c * 16 + 4 * at.a + at.b

    @pl.when(exists(at.a, at.b))
    def _():
        keys[0, own_slot, 0] = item_ref[...]
        for n in range(1, SP):
            k, i = divmod(n, 4)
            send(
                item_ref,
                keys.at[k, own_slot, i],
                zs.at[k],
                zr.at[k],
                (lax.rem(at.z - REL[n] + SP, SP), at.t),
            )

    gather = PlaneGather(at, keys, s1, r1, s2, r2, sd, rd)

    def chunk_here(k):
        @pl.when(exists(at.a, at.b))
        def _():
            arrived(keys.at[k, own_slot], zr.at[k])

    peak[...] = jnp.full(peak.shape, -1e30, jnp.float32)
    total[...] = jnp.zeros(total.shape, jnp.float32)
    accum[...] = jnp.zeros(accum.shape, jnp.float32)
    query = q_ref[...]
    lift = lift_ref[0, 0] * LOG2E

    def attend(k, g):
        block = keys[k, pl.ds(g * 16, OWNERS)].reshape(OWNERS * 4 * BLOCK, 640)
        ckv = block[:, :512]
        key = jnp.concatenate([nn(ckv, w_uk_ref[...]).astype(jnp.bfloat16), block[:, 512:]], axis=1)
        value = nt(w_uvt_ref[...], ckv).astype(jnp.bfloat16)
        score = nt(key, query) * (SCALE * LOG2E)
        extra = jnp.where(g == 1, lift, 0.0)
        score = jnp.concatenate([score[: 11 * 4 * BLOCK], score[11 * 4 * BLOCK :] + extra], axis=0)
        fresh = jnp.maximum(peak[...], jnp.max(score, axis=0, keepdims=True))
        probs = jnp.exp2(score - fresh)
        fade = jnp.exp2(peak[...] - fresh)
        peak[...] = fresh
        total[...] = total[...] * fade + jnp.sum(probs, axis=0, keepdims=True)
        accum[...] = accum[...] * fade + nn(value, probs.astype(jnp.bfloat16))

    @pl.when(exists(at.a, at.b))
    def _():
        arrived(keys.at[0, own_slot, pl.ds(1, 3)], zr.at[0])

    gather.first_start(0)
    gather.second_start(0, 0)

    def step(k, carry):
        last = k == CHUNKS

        @pl.when(jnp.logical_not(last))
        def _():
            gather.first_forward(k)
            gather.second_start(k, 1)
            gather.second_start(k, 2)

        @pl.when(k > 0)
        def _():
            attend(k - 1, at.c)

        @pl.when(jnp.logical_not(last))
        def _():
            gather.first_end(k)
            gather.second_start(k, 3)
            gather.second_forward(k, 0)

        @pl.when(k < CHUNKS - 1)
        def _():
            chunk_here(k + 1)
            gather.first_start(k + 1)

        @pl.when(k > 0)
        def _():
            gather.other_core(k - 1)
            attend(k - 1, 1 - at.c)

        @pl.when(jnp.logical_not(last))
        def _():
            gather.second_forward(k, 1)
            gather.second_forward(k, 2)
            gather.second_end(k, 0)
            gather.second_forward(k, 3)

        @pl.when(k < CHUNKS - 1)
        def _():
            gather.second_start(k + 1, 0)

        @pl.when(jnp.logical_not(last))
        def _():
            gather.second_end(k, 1)
            gather.second_end(k, 2)
            gather.second_end(k, 3)

        return carry

    lax.fori_loop(0, CHUNKS + 1, step, 0)

    rows = heads_in.shape[0]
    heads[...] = jnp.transpose(accum[...] / total[...]).astype(jnp.bfloat16)
    theirs = heads.at[pl.ds((1 - at.c) * rows, rows)]
    send(theirs, heads_in, hs, hr, at.partner())
    arrived(w_both, wr)
    arrived(heads_in, hr)
    mine = heads[pl.ds(at.c * rows, rows), :]
    other = heads_in[...]

    def product(p):
        columns = pl.ds(pl.multiple_of(p * 128, 128), 128)
        return nn(mine, w_out_ref[:, columns]) + nn(other, w_both[:, columns])

    for n, (dy, dx) in enumerate(FAR_FIRST):
        p = 4 * around(at.y, dy) + around(at.x, dx)
        pieces[n] = product(p).astype(jnp.bfloat16)
        send(pieces.at[n], pieces_in.at[n], ps, pr, (at.z, 2 * p + at.c))
    here = product(at.p)
    arrived(pieces_in, pr)
    for n in range(15):
        here = here + pieces_in[n].astype(jnp.float32)
    sums[...] = here
    send(sums, sums_in, xs, xr, at.partner())
    gate = gate_ref[...]

    def finish(value, start):
        value = jnp.where(at.c == 0, value[:, :64], value[:, 64:])
        where = pl.ds(start, rows)
        out_ref[where, :] = (latent_ref[where, :].astype(jnp.float32) + gate * value).astype(jnp.bfloat16)

    finish(here, at.c * rows)
    arrived(sums_in, xr)
    finish(sums_in[...], (1 - at.c) * rows)

    arrived(w_both, ws)
    arrived(heads_in, hs)
    arrived(pieces_in, ps)
    arrived(sums_in, xs)

    @pl.when(exists(at.a, at.b))
    def _():
        arrived(keys.at[0, 0, pl.ds(1, 3)], zs.at[0])
        for k in range(1, CHUNKS):
            arrived(keys.at[k, 0], zs.at[k])

    def sent(k, carry):
        gather.all_sent(k)
        return carry

    lax.fori_loop(0, CHUNKS, sent, 0)


def main(q, item, lift, latent, gate, w_uk, w_uvt, w_out):
    rows = latent.shape[0]
    vmem = pl.BlockSpec(memory_space=pltpu.VMEM)
    smem = pl.BlockSpec(memory_space=pltpu.SMEM)
    dma = pltpu.SemaphoreType.DMA
    return pl.pallas_call(
        main_kernel,
        out_shape=jax.ShapeDtypeStruct((rows, 64), jnp.bfloat16),
        in_specs=[vmem, vmem, smem, vmem, vmem, vmem, vmem, vmem],
        out_specs=vmem,
        scratch_shapes=[
            pltpu.VMEM((CHUNKS, 32, 4, BLOCK, 640), jnp.bfloat16),
            pltpu.VMEM((1, rows), jnp.float32),
            pltpu.VMEM((1, rows), jnp.float32),
            pltpu.VMEM((DV, rows), jnp.float32),
            pltpu.VMEM((DV, D), jnp.bfloat16),
            pltpu.VMEM((rows, DV), jnp.bfloat16),
            pltpu.VMEM((rows // 2, DV), jnp.bfloat16),
            pltpu.VMEM((15, rows // 2, 128), jnp.bfloat16),
            pltpu.VMEM((15, rows // 2, 128), jnp.bfloat16),
            pltpu.VMEM((rows // 2, 128), jnp.float32),
            pltpu.VMEM((rows // 2, 128), jnp.float32),
            dma((CHUNKS,)),
            dma((CHUNKS,)),
            dma((CHUNKS, 4)),
            dma((CHUNKS, 4)),
            dma((CHUNKS, 4, 4)),
            dma((CHUNKS, 4, 4)),
            dma((CHUNKS, 4)),
            dma((CHUNKS, 4)),
            dma,
            dma,
            dma,
            dma,
            dma,
            dma,
            dma,
            dma,
        ],
        compiler_params=pltpu.CompilerParams(
            collective_id=0, has_side_effects=True, vmem_limit_bytes=56 * 1024 * 1024
        ),
        name="main",
    )(q, item, lift, latent, gate, w_uk, w_uvt, w_out)


def tables(positions):
    row = (positions // GRID_W).astype(jnp.float32)
    col = (positions % GRID_W).astype(jnp.float32)
    half = ROPE // 2
    inverse = 1.0 / THETA ** (jnp.arange(0, half, 2, dtype=jnp.float32) / half)
    angle = jnp.concatenate([row[:, None] * inverse, col[:, None] * inverse], axis=-1)
    return (jnp.cos(angle), jnp.sin(angle))


def rotate(values, cosine, sine):
    shape = values.shape
    quarter = ROPE // 4
    parts = values.reshape(shape[:-1] + (2, 2, quarter))
    cosine = cosine.reshape((shape[0], 2, quarter))
    sine = sine.reshape((shape[0], 2, quarter))
    front, second = parts[..., 0, :], parts[..., 1, :]
    turned = jnp.stack([front * cosine - second * sine, front * sine + second * cosine], axis=-2)
    return turned.reshape(shape)


def modulated(values, sumsq, gain, modulation):
    scaled = values * lax.rsqrt(sumsq / D + EPS)[:, None] * gain
    return (scaled * (1.0 + modulation[1]) + modulation[0]).astype(jnp.bfloat16)


def low_norm(values, gain):
    scale = lax.rsqrt(jnp.mean(values * values, axis=-1, keepdims=True) + EPS)
    return (values * scale * gain).astype(jnp.bfloat16)


def per_device(
    latent, context, cond, cond_ctx, w_mod, g_norm, w_dq, w_dkv, w_kr, g_cq, g_ckv, w_uq, w_ukv, ctx_lift, w_out
):
    rows = latent.shape[0]
    signal = jnp.stack(
        [jax.nn.silu(cond.astype(jnp.float32)), jax.nn.silu(cond_ctx.astype(jnp.float32))]
    ).astype(jnp.bfloat16)
    partial_mod = nn(signal, w_mod.reshape(w_mod.shape[0], -1))
    modulation = lax.psum(partial_mod.reshape(2, 3, -1), "sp")
    lat_f = latent.astype(jnp.float32)
    ctx_f = context.astype(jnp.float32)
    squares = lax.psum(jnp.concatenate([jnp.sum(lat_f * lat_f, axis=1), jnp.sum(ctx_f * ctx_f, axis=1)]), "tp")
    lat_h = modulated(lat_f, squares[:rows], g_norm, modulation[0])
    ctx_h = modulated(ctx_f, squares[rows:], g_norm, modulation[1])
    whole = nn(jnp.concatenate([lat_h, ctx_h], axis=0), jnp.concatenate([w_dq, w_dkv, w_kr], axis=1))
    whole = lax.psum(whole, "tp")
    positions = lax.axis_index("sp") * rows + jnp.arange(rows, dtype=jnp.int32)
    cosine, sine = tables(positions)
    cq_n = low_norm(whole[:rows, :512], g_cq)
    ckv_n = low_norm(whole[:, 512:1024], g_ckv)
    rot = whole[:, 1024:]
    rot = jnp.concatenate([rotate(rot[:rows], cosine, sine), rot[rows:]], axis=0).astype(jnp.bfloat16)
    kv = jnp.concatenate([ckv_n, rot, jnp.zeros_like(rot)], axis=1)
    query = nn(cq_n, w_uq[:, 0, :])
    query = jnp.concatenate(
        [query[:, :NOPE], rotate(query[:, NOPE:], cosine, sine), jnp.zeros((rows, 64), jnp.float32)], axis=1
    ).astype(jnp.bfloat16)
    at = Place()
    index = jnp.minimum(13 * at.c + 4 * at.a + at.b, 25)
    item = lax.dynamic_slice_in_dim(kv, index * BLOCK, BLOCK, axis=0)
    up = w_ukv[:, 0, :]
    return main(
        query,
        item,
        ctx_lift.reshape(1, 1),
        latent,
        modulation[0, 2][None, :],
        up[:, :NOPE],
        up[:, NOPE:].T,
        w_out[0],
    )


def solution(mesh):
    return jax.shard_map(
        per_device,
        mesh=mesh,
        in_specs=(
            P("sp", "tp"),
            P("sp", "tp"),
            P("sp"),
            P("sp"),
            P("sp", None, "tp"),
            P("tp"),
            P("tp", None),
            P("tp", None),
            P("tp", None),
            P(),
            P(),
            P(None, "tp", None),
            P(None, "tp", None),
            P("tp"),
            P("tp", None, None),
        ),
        out_specs=P("sp", "tp"),
        check_vma=False,
    )
```

time: 288 us -> 353 us (1.23)
  Pallas kernels: 0 us -> 90.5 us
  waiting for transfers between devices: 53.7 us -> 137 us
  local copies, waits for them, and re-layouts: 64.1 us -> 4.71 us
  starting transfers between devices: 27 us -> 0.01 us
  matrix products: 22 us -> 5.09 us
  other arithmetic: 12.2 us -> 8 us
    psum x0 -> x1, waiting for transfers between devices: none -> 137 us  [per_device(): whole = lax.psum(whole, 'tp')]
    psum x0 -> x2, blocking collectives: none -> 93.1 us  [the longest x1 68.9 us: per_device(): lax.psum(jnp.concatenate([jnp.sum(lat_f * lat_f, axis=1), jnp.sum(ctx_f *...]
    pallas_call x0 -> x1, Pallas kernels: none -> 90.5 us  [main(): pl.pallas_call(main_kernel, out_shape=jax.ShapeDtypeStruct((rows, 64), jn...]
    all_to_all x5 -> x0, blocking collectives: 66.2 us -> none  [the longest x1 19.9 us: sum_by_axis(): lax.all_to_all(nearer.astype(jnp.bfloat16), far, split_axis=0, concat_axi...]
    all_to_all x3 -> x0, waiting for transfers between devices: 29.9 us -> none  [copy_for_each(): lax.all_to_all(jnp.broadcast_to(shard[None], (length, *shard.shape)), axi...]
    all_to_all x3 -> x0, starting transfers between devices: 27 us -> none  [copy_for_each(): lax.all_to_all(jnp.broadcast_to(shard[None], (length, *shard.shape)), axi...]
    all_gather x1 -> x0, blocking collectives: 26 us -> none  [in_one_piece(): filled, at, outs = (lax.all_gather(both, axis, axis=dim, tiled=True), 0, [])]
    slice x28 -> x6, local copies, waits for them, and re-layouts: 25.5 us -> 0.9 us  [the longest x1 0.75 us: per_device(): up[:, :NOPE]]
  transfers between devices with their start and end apart: 4 -> 1, of which waited for: 4 -> 1; matrix products, arithmetic and copies ran while one was open for 3% -> 1% of each run, Pallas kernels for 0% -> 0%
where the time goes in v1:
time: 353 us; the launch traced here: 352 us
  waiting for transfers between devices  137 us (39%)
  blocking collectives  93.1 us (26%)
  Pallas kernels  90.5 us (26%)
  between operations  14.3 us (4%)
  other arithmetic  8 us (2%)
  matrix products  5.09 us (1%)
  local copies, waits for them, and re-layouts  4.71 us (1%)
    psum x1, waiting for transfers between devices, per_device(): whole = lax.psum(whole, 'tp')  137 us
    pallas_call x1, Pallas kernels, main(): pl.pallas_call(main_kernel, out_shape=jax.ShapeDtypeStruct((rows, 64), jn...  90.5 us
    psum x1, blocking collectives, per_device(): lax.psum(jnp.concatenate([jnp.sum(lat_f * lat_f, axis=1), jnp.sum(ctx_f *...  68.9 us
    psum x1, blocking collectives, per_device(): modulation = lax.psum(partial_mod.reshape(2, 3, -1), 'sp')  24.2 us
  transfers between devices with their start and end apart: 1, of which 1 were waited for; matrix products, arithmetic and copies ran while one was open for 1% of the time, Pallas kernels for 0%

profile of v1, /device:TPU:1, one launch (start us, length us, event | category | flops | bytes accessed | tf_op | source)
XLA Modules:
  0.0 352.1 jit_solution(8030036940642027173)
XLA Ops:
  6.5 0.9 fusion.10
  7.4 0.8 fusion.25
  8.2 68.9 %psum.21 = f32[416]{0:T(512)S(1)} all-reduce(f32[416]{0:T(512)S(1)} %pad_maximum_fusion.3), channel_id=1, replica_groups=mesh['sp'=16,'tp'=32] {'tp'}, use_global_device_ids=true, to_apply=%region_2.3 | all-reduce | flops 416 | bytes 3328 | tf_op jit(solution)/shard_map/psum | solution.py:496
  77.1 0.7 convert_bitcast_fusion
  77.8 0.9 fusion.18
  78.7 24.2 %psum.22 = f32[2,3,64]{2,0,1:T(2,128)S(1)} all-reduce(f32[2,3,64]{2,0,1:T(2,128)S(1)} %fusion.18), channel_id=1, replica_groups=mesh['sp'=16,'tp'=32] {'sp'}, use_global_device_ids=true, to_apply=%region_3.4 | all-reduce | flops 384 | bytes 3072 | tf_op jit(solution)/shard_map/psum | solution.py:493
  102.9 0.5 slice_bitcast_fusion.1
  103.5 0.8 fusion.29
  104.3 0.9 fusion.14
  105.3 2.6 fusion.4
  108.1 0.7 copy.40.latent_ref
  108.9 0.1 copy.39
  109.0 0.7 slice_bitcast_fusion
  109.7 0.7 copy.41.w_uk_ref
  111.2 136.5 %all-reduce.2.cloned.1.call-done = f32[416,1088]{1,0:T(8,128)} async-done(((f32[416,1088]{1,0:T(8,128)}), f32[416,1088]{1,0:T(8,128)}) %all-reduce.2.cloned.1.call-update) | async-done | bytes 1810448 | tf_op jit(solution)/shard_map/psum | solution.py:500
  247.7 1.4 multiply_reduce_fusion.1
  249.2 1.5 fusion
  250.9 0.2 subtract_convert_fusion
  251.3 0.2 multiply_reduce_fusion
  251.7 0.7 maximum_maximum_fusion.q_ref
  252.4 0.1 multiply_convert_fusion
  252.6 0.6 fusion.24.item_ref
  253.2 90.5 %main.1 = bf16[384,64]{1,0:T(8,128)(2,1)} custom-call(bf16[384,256]{1,0:T(8,128)(2,1)} %maximum_maximum_fusion.q_ref, bf16[16,640]{1,0:T(8,128)(2,1)} %fusion.24.item_ref, f32[1,1]{1,0:T(1,128)} %bitcast.40.lift_ref, bf16[384,64]{1,0:T(8,128)(2,1)} %copy.40.latent_ref, f32[1,64]{1,0:T(1,128)} %get-tuple-element.13.gate_ref, bf16[512,128]{1,0:T(8,128)(2,1)} %copy.41.w_uk_ref, ...), custom_call_target="tpu_custom_call" | custom-call | tf_op jit(solution)/shard_map/main/pallas_call | solution.py:414
  343.7 1.6 copy.42
  (36 shorter events, 1.0 us)
Async XLA Ops:
  6.5 242.6 %copy-start = (bf16[512,1,192]{0,2,1:T(8,128)(2,1)S(1)}, bf16[512,1,192]{0,2,1:T(8,128)(2,1)}, u32[]{:S(2)}) copy-start(bf16[512,1,192]{0,2,1:T(8,128)(2,1)} %param.26) | copy-start | bytes 589828
  6.5 241.2 %all-reduce.2.cloned.1.call-start = ((), (), s32[]{:S(2)}) async-start(), calls=%async_computation | async-start | bytes 3833856 | tf_op jit(solution)/shard_map/psum | solution.py:500
  105.2 2.9 copy-start.2
  105.3 3.6 %copy-start.3 = (bf16[512,1,256]{2,0,1:T(8,128)(2,1)S(1)}, bf16[512,1,256]{2,0,1:T(8,128)(2,1)}, u32[]{:S(2)}) copy-start(bf16[512,1,256]{2,0,1:T(8,128)(2,1)} %param.27) | copy-start | bytes 786436
  107.9 141.3 %copy-start.4 = (f32[512]{0:T(512)S(1)}, f32[512]{0:T(512)}, u32[]{:S(2)}) copy-start(f32[512]{0:T(512)} %param.24) | copy-start | bytes 6148
  247.7 3.0 copy-start.1
  250.7 1.7 copy-start.5
Sparse Core Ops, SparseCore 0:
  108.0 139.6 all-reduce.1

commit v2 on v1

v2 whole, which is shorter than its diff:
```python
import numpy as np

import jax
import jax.numpy as jnp
from jax import lax
from jax.experimental import pallas as pl
from jax.experimental.pallas import tpu as pltpu

from jax.sharding import PartitionSpec as P

MESH = pl.DeviceIdType.MESH
D = 2048
NOPE = 128
ROPE = 64
DV = 128
GRID_W = 64
EPS = 1e-06
THETA = 10000.0
LOG2E = 1.4426950408889634
SCALE = (NOPE + ROPE) ** (-0.5)

BLOCK = 16
OWNERS = 13
SP = 16
CHUNKS = 4
REL = (0, 1, -1, 2, -2, 3, -3, 4, -4, 5, -5, 6, -6, 7, -7, 8)
FAR_FIRST = tuple(
    sorted(
        [(dy, dx) for dy in range(4) for dx in range(4) if dy or dx],
        key=lambda o: -(min(o[0], 4 - o[0]) + min(o[1], 4 - o[1])),
    )
)


def nn(lhs, rhs):
    return jnp.dot(lhs, rhs, preferred_element_type=jnp.float32)


def nt(lhs, rhs):
    return lax.dot_general(lhs, rhs, (((1,), (1,)), ((), ())), preferred_element_type=jnp.float32)


class Place:
    def __init__(self):
        self.z = lax.axis_index("sp")
        self.t = lax.axis_index("tp")
        self.p = lax.div(self.t, 2)
        self.c = lax.rem(self.t, 2)
        self.y = lax.div(self.p, 4)
        self.x = lax.rem(self.p, 4)
        self.a = self.x * (1 - self.c) + self.y * self.c
        self.b = self.y * (1 - self.c) + self.x * self.c

    def dev(self, a, b):
        p = (4 * b + a) * (1 - self.c) + (4 * a + b) * self.c
        return (self.z, 2 * p + self.c)

    def partner(self):
        return (self.z, 2 * self.p + 1 - self.c)


def around(i, by):
    return lax.rem(i + by + 4, 4)


def exists(a, b):
    return 4 * a + b < OWNERS


def send(src, dst, send_sem, recv_sem, device):
    copy = pltpu.make_async_remote_copy(
        src_ref=src,
        dst_ref=dst,
        send_sem=send_sem,
        recv_sem=recv_sem,
        device_id=device,
        device_id_type=MESH,
    )
    copy.start()


def arrived(ref, sem):
    pltpu.make_async_copy(ref, ref, sem).wait()


class PlaneGather:
    def __init__(self, at, buf, owners, part, sems):
        s1, r1, s2, r2, sd, rd = sems
        self.at = at
        self.buf = buf
        self.owners = owners
        self.part = part
        self.s1, self.r1, self.s2, self.r2, self.sd, self.rd = s1, r1, s2, r2, sd, rd
        self.offsets = (0, -1, 1, 2)

    def exists(self, a, b):
        return 4 * a + b < self.owners

    def slot(self, k, a, b):
        return self.buf.at[k, self.at.c * 16 + 4 * a + b]

    def half(self, k, a, b, h):
        return self.buf.at[k, self.at.c * 16 + 4 * a + b, pl.ds(self.part * h, self.part)]

    def first_start(self, k):
        at = self.at

        @pl.when(self.exists(at.a, at.b))
        def _():
            own = self.slot(k, at.a, at.b)
            send(own, own, self.s1.at[k, 0], self.r1.at[k, 0], at.dev(around(at.a, 1), at.b))
            send(own, own, self.s1.at[k, 1], self.r1.at[k, 1], at.dev(around(at.a, -1), at.b))

    def first_forward(self, k):
        at = self.at
        for role, by in ((0, -1), (1, 1)):
            a = around(at.a, by)

            @pl.when(self.exists(a, at.b))
            def _():
                arrived(self.slot(k, a, at.b), self.r1.at[k, role])
                part = self.half(k, a, at.b, role)
                send(part, part, self.s1.at[k, 2 + role], self.r1.at[k, 2 + role], at.dev(around(at.a, -by), at.b))

    def first_end(self, k):
        at = self.at
        a = around(at.a, 2)

        @pl.when(self.exists(a, at.b))
        def _():
            for role in (0, 1):
                arrived(self.half(k, a, at.b, role), self.r1.at[k, 2 + role])

    def second_start(self, k, j):
        at = self.at
        a = around(at.a, self.offsets[j])

        @pl.when(self.exists(a, at.b))
        def _():
            own = self.slot(k, a, at.b)
            send(own, own, self.s2.at[k, j, 0], self.r2.at[k, j, 0], at.dev(at.a, around(at.b, 1)))
            send(own, own, self.s2.at[k, j, 1], self.r2.at[k, j, 1], at.dev(at.a, around(at.b, -1)))

    def second_forward(self, k, j):
        at = self.at
        a = around(at.a, self.offsets[j])
        for role, by in ((0, -1), (1, 1)):
            b = around(at.b, by)

            @pl.when(self.exists(a, b))
            def _():
                arrived(self.slot(k, a, b), self.r2.at[k, j, role])
                part = self.half(k, a, b, role)
                send(part, part, self.s2.at[k, j, 2 + role], self.r2.at[k, j, 2 + role], at.dev(at.a, around(at.b, -by)))

    def second_end(self, k, j):
        at = self.at
        a = around(at.a, self.offsets[j])
        b = around(at.b, 2)

        @pl.when(self.exists(a, b))
        def _():
            for role in (0, 1):
                arrived(self.half(k, a, b, role), self.r2.at[k, j, 2 + role])

        row = self.buf.at[k, pl.ds(at.c * 16 + 4 * a, 4)]
        send(row, row, self.sd.at[k, j], self.rd.at[k, j], at.partner())

    def other_core(self, k):
        at = self.at
        for j in range(4):
            a = around(at.b, self.offsets[j])
            arrived(self.buf.at[k, pl.ds((1 - at.c) * 16 + 4 * a, 4)], self.rd.at[k, j])

    def all_sent(self, k):
        at = self.at
        own = self.slot(k, 0, 0)
        part = self.half(k, 0, 0, 0)

        @pl.when(self.exists(at.a, at.b))
        def _():
            arrived(own, self.s1.at[k, 0])
            arrived(own, self.s1.at[k, 1])

        for role, by in ((0, -1), (1, 1)):

            @pl.when(self.exists(around(at.a, by), at.b))
            def _():
                arrived(part, self.s1.at[k, 2 + role])

        for j in range(4):
            a = around(at.a, self.offsets[j])

            @pl.when(self.exists(a, at.b))
            def _():
                arrived(own, self.s2.at[k, j, 0])
                arrived(own, self.s2.at[k, j, 1])

            for role, by in ((0, -1), (1, 1)):

                @pl.when(self.exists(a, around(at.b, by)))
                def _():
                    arrived(part, self.s2.at[k, j, 2 + role])

            arrived(self.buf.at[k, pl.ds(0, 4)], self.sd.at[k, j])


def swapped(values):
    lane = lax.broadcasted_iota(jnp.int32, values.shape, 1)
    return jnp.where(lax.rem(lane, 32) < 16, pltpu.roll(values, 112, 1), pltpu.roll(values, 16, 1))


def low_norm(values, gain):
    scale = lax.rsqrt(jnp.mean(values * values, axis=-1, keepdims=True) + EPS)
    return (values * scale * gain).astype(jnp.bfloat16)


def main_kernel(
    latent_ref,
    context_ref,
    mod_ref,
    g_norm_ref,
    w_dq_ref,
    w_dkv_ref,
    w_kr_ref,
    g_cq_ref,
    g_ckv_ref,
    lift_ref,
    row_cos_ref,
    row_sin_ref,
    col_cos_ref,
    col_sin_ref,
    w_uq_hbm,
    w_ukv_hbm,
    w_out_hbm,
    out_ref,
    mod_in,
    mod_mine,
    mod_all,
    x_all,
    h_all,
    w_down,
    compressed,
    item,
    w_uq,
    w_up,
    w_uvt,
    w_out,
    query,
    keys,
    peak,
    total,
    accum,
    w_other,
    heads,
    heads_in,
    pieces,
    pieces_in,
    sums,
    sums_in,
    ms,
    mr,
    as_,
    ar,
    vs,
    vr,
    zs,
    zr,
    *rest,
):
    down_sems, cq_sems, key_sems = rest[0:6], rest[6:12], rest[12:18]
    ws, wr, hs, hr, ps, pr, xs, xr, l1, l2, l3 = rest[18:]
    at = Place()
    owner = exists(at.a, at.b)
    own_slot = at.c * 16 + 4 * at.a + at.b
    own_item = jnp.minimum(at.c * OWNERS + 4 * at.a + at.b, 25)
    in_context = own_item >= 24

    barrier = pltpu.get_barrier_semaphore()

    def greet_z(i, carry):
        pl.semaphore_signal(barrier, inc=1, device_id=(lax.rem(at.z + i, SP), at.t), device_id_type=MESH)
        return carry

    def greet_plane(i, carry):
        pl.semaphore_signal(barrier, inc=1, device_id=(at.z, lax.rem(at.t + i, 32)), device_id_type=MESH)
        return carry

    lax.fori_loop(1, SP, greet_z, 0)
    lax.fori_loop(1, 32, greet_plane, 0)

    loads = [
        pltpu.make_async_copy(w_uq_hbm, w_uq, l1),
        pltpu.make_async_copy(w_ukv_hbm, w_up, l2),
        pltpu.make_async_copy(w_out_hbm, w_out, l3),
    ]
    for load in loads:
        load.start()

    half_rows = w_dq_ref.shape[0] // 2
    for h in range(2):
        rows = pl.ds(h * half_rows, half_rows)
        w_down[0, own_slot, h, :, 0:512] = w_dq_ref[rows, :]
        w_down[0, own_slot, h, :, 512:1024] = w_dkv_ref[rows, :]
        w_down[0, own_slot, h, :, 1024:1152] = jnp.concatenate(
            [w_kr_ref[rows, :], jnp.zeros((half_rows, 64), jnp.bfloat16)], axis=1
        )
    mod_mine[...] = jnp.zeros(mod_mine.shape, jnp.float32)
    peak[...] = jnp.full(peak.shape, -1e30, jnp.float32)
    total[...] = jnp.zeros(total.shape, jnp.float32)
    accum[...] = jnp.zeros(accum.shape, jnp.float32)

    pl.semaphore_wait(barrier, 46)

    for n in range(1, SP):
        send(mod_ref, mod_in.at[n - 1], ms, mr, (lax.rem(at.z - REL[n] + SP, SP), at.t))

    down = PlaneGather(at, w_down, 16, 1, down_sems)
    down.first_start(0)
    down.second_start(0, 0)

    def give(i, source):
        c = lax.div(i, OWNERS)
        l = i - c * OWNERS
        a, b = lax.div(l, 4), lax.rem(l, 4)
        t = 2 * ((4 * b + a) * (1 - c) + (4 * a + b) * c) + c

        @pl.when(t != at.t)
        def _():
            send(source, x_all.at[own_slot], as_, ar, (at.z, t))

        @pl.when(t == at.t)
        def _():
            x_all[own_slot] = source[...]

    def give_latent(i, carry):
        give(i, latent_ref.at[pl.ds(pl.multiple_of(i * BLOCK, BLOCK), BLOCK)])
        return carry

    lax.fori_loop(0, 24, give_latent, 0)
    for i in (24, 25):
        give(jnp.int32(i), context_ref.at[pl.ds((i - 24) * BLOCK, BLOCK)])

    down.first_forward(0)
    down.second_start(0, 1)
    down.second_start(0, 2)
    loads[2].wait()
    send(w_out, w_other, ws, wr, at.partner())
    loads[1].wait()
    w_uvt[...] = jnp.transpose(w_up[:, NOPE:].astype(jnp.float32)).astype(jnp.bfloat16)
    down.first_end(0)
    down.second_start(0, 3)
    down.second_forward(0, 0)

    arrived(mod_in, mr)
    mod = mod_ref[...]
    for n in range(SP - 1):
        mod = mod + mod_in[n]
    mod_mine[:, 0:384] = mod
    mod_mine[:, 384:448] = g_norm_ref[...]
    mod_all[own_slot] = mod_mine[...]

    def tell(i, carry):
        send(mod_mine, mod_all.at[own_slot], vs, vr, (at.z, lax.rem(at.t + i, 32)))
        return carry

    lax.fori_loop(1, 32, tell, 0)

    for j in (1, 2, 3):
        down.second_forward(0, j)
    loads[0].wait()
    for j in range(4):
        down.second_end(0, j)

    @pl.when(owner)
    def _():
        arrived(x_all.at[pl.ds(0, 31)], ar)

    x = x_all[...].astype(jnp.float32)
    squares = jnp.sum(jnp.sum(x * x, axis=0), axis=1, keepdims=True)
    norm = lax.rsqrt(squares / D + EPS)
    arrived(mod_all.at[pl.ds(0, 31)], vr)
    for s in range(0, 32, 2):
        pair = []
        for slot in (s, s + 1):
            m = mod_all[slot]
            shift = jnp.where(in_context, m[:, 192:256], m[:, 0:64])
            scale = jnp.where(in_context, m[:, 256:320], m[:, 64:128])
            pair.append((x[slot] * norm * m[:, 384:448] * (1.0 + scale) + shift).astype(jnp.bfloat16))
        h_all[:, s * 64 : s * 64 + 128] = jnp.concatenate(pair, axis=1)
    down.other_core(0)
    low = nn(h_all[...], w_down[0].reshape(D, 1152))

    first_row = at.z * 6
    item_row = first_row + lax.div(jnp.minimum(own_item, 23), 4)
    item_col = pl.ds(pl.multiple_of(lax.rem(own_item, 4) * BLOCK, BLOCK), BLOCK)
    item_cos = jnp.where(in_context, 1.0, row_cos_ref[pl.ds(item_row, 1), :] + col_cos_ref[item_col, :])
    item_sin = jnp.where(in_context, 0.0, row_sin_ref[pl.ds(item_row, 1), :] + col_sin_ref[item_col, :])
    rotary = low[:, 1024:1152]
    rotary = rotary * item_cos + swapped(rotary) * item_sin
    item[:, 0:512] = low_norm(low[:, 512:1024], g_ckv_ref[...])
    item[:, 512:640] = rotary.astype(jnp.bfloat16)
    cq = low_norm(low[:, 0:512], g_cq_ref[...])
    compressed[0, own_slot, 0] = cq[:, 0:256]
    compressed[0, own_slot, 1] = cq[:, 256:512]

    @pl.when(owner)
    def _():
        keys[0, own_slot, 0] = item[...]
        for n in range(1, SP):
            k, i = divmod(n, 4)
            send(
                item,
                keys.at[k, own_slot, i],
                zs.at[k],
                zr.at[k],
                (lax.rem(at.z - REL[n] + SP, SP), at.t),
            )

    ask = PlaneGather(at, compressed, OWNERS, 1, cq_sems)
    gather = PlaneGather(at, keys, OWNERS, 2, key_sems)
    ask.first_start(0)
    ask.second_start(0, 0)
    ask.first_forward(0)
    ask.second_start(0, 1)
    ask.second_start(0, 2)

    def chunk_here(k):
        @pl.when(owner)
        def _():
            arrived(keys.at[k, own_slot], zr.at[k])

    lift = lift_ref[0, 0] * LOG2E

    def attend(k, g):
        block = keys[k, pl.ds(g * 16, OWNERS)].reshape(OWNERS * 4 * BLOCK, 640)
        ckv = block[:, :512]
        key = jnp.concatenate([nn(ckv, w_up[:, :NOPE]).astype(jnp.bfloat16), block[:, 512:]], axis=1)
        value = nt(w_uvt[...], ckv).astype(jnp.bfloat16)
        score = nt(key, query[...]) * (SCALE * LOG2E)
        extra = jnp.where(g == 1, lift, 0.0)
        score = jnp.concatenate([score[: 11 * 4 * BLOCK], score[11 * 4 * BLOCK :] + extra], axis=0)
        fresh = jnp.maximum(peak[...], jnp.max(score, axis=0, keepdims=True))
        probs = jnp.exp2(score - fresh)
        fade = jnp.exp2(peak[...] - fresh)
        peak[...] = fresh
        total[...] = total[...] * fade + jnp.sum(probs, axis=0, keepdims=True)
        accum[...] = accum[...] * fade + nn(value, probs.astype(jnp.bfloat16))

    @pl.when(owner)
    def _():
        arrived(keys.at[0, own_slot, pl.ds(1, 3)], zr.at[0])

    gather.first_start(0)
    ask.first_end(0)
    ask.second_start(0, 3)
    for j in range(4):
        ask.second_forward(0, j)
    gather.second_start(0, 0)
    for j in range(4):
        ask.second_end(0, j)

    def make_query():
        ask.other_core(0)
        pieces = [compressed[0, pl.ds(16 * c, 13 - 2 * c), h] for c in range(2) for h in range(2)]
        pieces = [piece.reshape(-1, 256) for piece in pieces]
        cq = jnp.concatenate(
            [jnp.concatenate(pieces[0:2], axis=1), jnp.concatenate(pieces[2:4], axis=1)], axis=0
        )
        query[:, 0:NOPE] = nn(cq, w_uq[:, 0:NOPE]).astype(jnp.bfloat16)
        turn = nn(cq, w_uq[:, NOPE:])
        turn = jnp.concatenate([turn, jnp.zeros_like(turn)], axis=1)
        for r in range(6):
            values = turn[64 * r : 64 * r + 64]
            cosine = row_cos_ref[pl.ds(first_row + r, 1), :] + col_cos_ref[...]
            sine = row_sin_ref[pl.ds(first_row + r, 1), :] + col_sin_ref[...]
            query[64 * r : 64 * r + 64, NOPE:] = (values * cosine + swapped(values) * sine).astype(jnp.bfloat16)

    def step(k, carry):
        last = k == CHUNKS

        @pl.when(jnp.logical_not(last))
        def _():
            gather.first_forward(k)
            gather.second_start(k, 1)
            gather.second_start(k, 2)

        @pl.when(k == 0)
        def _():
            make_query()

        @pl.when(k > 0)
        def _():
            attend(k - 1, at.c)

        @pl.when(jnp.logical_not(last))
        def _():
            gather.first_end(k)
            gather.second_start(k, 3)
            gather.second_forward(k, 0)

        @pl.when(k < CHUNKS - 1)
        def _():
            chunk_here(k + 1)
            gather.first_start(k + 1)

        @pl.when(k > 0)
        def _():
            gather.other_core(k - 1)
            attend(k - 1, 1 - at.c)

        @pl.when(jnp.logical_not(last))
        def _():
            gather.second_forward(k, 1)
            gather.second_forward(k, 2)
            gather.second_end(k, 0)
            gather.second_forward(k, 3)

        @pl.when(k < CHUNKS - 1)
        def _():
            gather.second_start(k + 1, 0)

        @pl.when(jnp.logical_not(last))
        def _():
            gather.second_end(k, 1)
            gather.second_end(k, 2)
            gather.second_end(k, 3)

        return carry

    lax.fori_loop(0, CHUNKS + 1, step, 0)

    rows = heads_in.shape[0]
    heads[...] = jnp.transpose(accum[...] / total[...]).astype(jnp.bfloat16)
    theirs = heads.at[pl.ds((1 - at.c) * rows, rows)]
    send(theirs, heads_in, hs, hr, at.partner())
    arrived(w_other, wr)
    arrived(heads_in, hr)
    mine = heads[pl.ds(at.c * rows, rows), :]
    other = heads_in[...]

    def product(p):
        columns = pl.ds(pl.multiple_of(p * 128, 128), 128)
        return nn(mine, w_out[:, columns]) + nn(other, w_other[:, columns])

    for n, (dy, dx) in enumerate(FAR_FIRST):
        p = 4 * around(at.y, dy) + around(at.x, dx)
        pieces[n] = product(p).astype(jnp.bfloat16)
        send(pieces.at[n], pieces_in.at[n], ps, pr, (at.z, 2 * p + at.c))
    here = product(at.p)
    arrived(pieces_in, pr)
    for n in range(15):
        here = here + pieces_in[n].astype(jnp.float32)
    sums[...] = here
    send(sums, sums_in, xs, xr, at.partner())
    gate = mod_mine[:, 128:192]

    def finish(value, start):
        value = jnp.where(at.c == 0, value[:, :64], value[:, 64:])
        where = pl.ds(start, rows)
        out_ref[where, :] = (latent_ref[where, :].astype(jnp.float32) + gate * value).astype(jnp.bfloat16)

    finish(here, at.c * rows)
    arrived(sums_in, xr)
    finish(sums_in[...], (1 - at.c) * rows)

    arrived(mod_in, ms)
    arrived(mod_all.at[pl.ds(0, 31)], vs)
    arrived(w_other, ws)
    arrived(heads_in, hs)
    arrived(pieces_in, ps)
    arrived(sums_in, xs)

    @pl.when(owner)
    def _():
        arrived(x_all.at[pl.ds(0, 25)], as_)
        arrived(keys.at[0, 0, pl.ds(1, 3)], zs.at[0])
        for k in range(1, CHUNKS):
            arrived(keys.at[k, 0], zs.at[k])

    @pl.when(jnp.logical_not(owner))
    def _():
        arrived(x_all.at[pl.ds(0, 26)], as_)

    down.all_sent(0)
    ask.all_sent(0)

    def sent(k, carry):
        gather.all_sent(k)
        return carry

    lax.fori_loop(0, CHUNKS, sent, 0)


def gather_sems(chunks):
    dma = pltpu.SemaphoreType.DMA
    return [
        dma((chunks, 4)),
        dma((chunks, 4)),
        dma((chunks, 4, 4)),
        dma((chunks, 4, 4)),
        dma((chunks, 4)),
        dma((chunks, 4)),
    ]


def turn_tables():
    half = ROPE // 2
    inverse = (np.float32(1.0) / np.float32(THETA) ** (np.arange(0, half, 2, dtype=np.float32) / np.float32(half))).astype(
        np.float32
    )

    def table(count, start):
        angle = (np.arange(count, dtype=np.float32)[:, None] * inverse).astype(np.float32)
        cosine, sine = np.cos(angle), np.sin(angle)
        whole_cos = np.zeros((count, 128), np.float32)
        whole_sin = np.zeros((count, 128), np.float32)
        whole_cos[:, start : start + 32] = np.concatenate([cosine, cosine], axis=1)
        whole_sin[:, start : start + 32] = np.concatenate([-sine, sine], axis=1)
        return whole_cos, whole_sin

    return table(6144 // GRID_W, 0) + table(GRID_W, 32)


def per_device(
    latent, context, cond, cond_ctx, w_mod, g_norm, w_dq, w_dkv, w_kr, g_cq, g_ckv, w_uq, w_ukv, ctx_lift, w_out
):
    rows = latent.shape[0]
    signal = jnp.stack(
        [jax.nn.silu(cond.astype(jnp.float32)), jax.nn.silu(cond_ctx.astype(jnp.float32))]
    ).astype(jnp.bfloat16)
    partial_mod = nn(signal, w_mod.reshape(w_mod.shape[0], -1)).reshape(1, 384)
    vmem = pl.BlockSpec(memory_space=pltpu.VMEM)
    smem = pl.BlockSpec(memory_space=pltpu.SMEM)
    hbm = pl.BlockSpec(memory_space=pltpu.HBM)
    dma = pltpu.SemaphoreType.DMA
    bf16, f32 = jnp.bfloat16, jnp.float32
    return pl.pallas_call(
        main_kernel,
        out_shape=jax.ShapeDtypeStruct((rows, 64), bf16),
        in_specs=[vmem] * 9 + [smem] + [vmem] * 4 + [hbm] * 3,
        out_specs=vmem,
        scratch_shapes=[
            pltpu.VMEM((SP - 1, 1, 384), f32),
            pltpu.VMEM((1, 512), f32),
            pltpu.VMEM((32, 1, 512), f32),
            pltpu.VMEM((32, BLOCK, 64), bf16),
            pltpu.VMEM((BLOCK, D), bf16),
            pltpu.VMEM((1, 32, 2, 32, 1152), bf16),
            pltpu.VMEM((1, 32, 2, BLOCK, 256), bf16),
            pltpu.VMEM((BLOCK, 640), bf16),
            pltpu.VMEM((512, NOPE + ROPE), bf16),
            pltpu.VMEM((512, NOPE + DV), bf16),
            pltpu.VMEM((DV, 512), bf16),
            pltpu.VMEM((DV, D), bf16),
            pltpu.VMEM((rows, 256), bf16),
            pltpu.VMEM((CHUNKS, 32, 4, BLOCK, 640), bf16),
            pltpu.VMEM((1, rows), f32),
            pltpu.VMEM((1, rows), f32),
            pltpu.VMEM((DV, rows), f32),
            pltpu.VMEM((DV, D), bf16),
            pltpu.VMEM((rows, DV), bf16),
            pltpu.VMEM((rows // 2, DV), bf16),
            pltpu.VMEM((15, rows // 2, 128), bf16),
            pltpu.VMEM((15, rows // 2, 128), bf16),
            pltpu.VMEM((rows // 2, 128), f32),
            pltpu.VMEM((rows // 2, 128), f32),
            dma,
            dma,
            dma,
            dma,
            dma,
            dma,
            dma((CHUNKS,)),
            dma((CHUNKS,)),
            *gather_sems(1),
            *gather_sems(1),
            *gather_sems(CHUNKS),
            *[dma] * 11,
        ],
        compiler_params=pltpu.CompilerParams(
            collective_id=0, has_side_effects=True, vmem_limit_bytes=56 * 1024 * 1024
        ),
        name="main",
    )(
        latent,
        context,
        partial_mod,
        g_norm[None, :],
        w_dq,
        w_dkv,
        w_kr,
        g_cq[None, :],
        g_ckv[None, :],
        ctx_lift.reshape(1, 1),
        *turn_tables(),
        w_uq[:, 0, :],
        w_ukv[:, 0, :],
        w_out[0],
    )


def solution(mesh):
    return jax.shard_map(
        per_device,
        mesh=mesh,
        in_specs=(
            P("sp", "tp"),
            P("sp", "tp"),
            P("sp"),
            P("sp"),
            P("sp", None, "tp"),
            P("tp"),
            P("tp", None),
            P("tp", None),
            P("tp", None),
            P(),
            P(),
            P(None, "tp", None),
            P(None, "tp", None),
            P("tp"),
            P("tp", None, None),
        ),
        out_specs=P("sp", "tp"),
        check_vma=False,
    )
```

time: 353 us -> 124 us (0.35)
  waiting for transfers between devices: 137 us -> 0 us
  blocking collectives: 93.1 us -> 0 us
  Pallas kernels: 90.5 us -> 118 us
  between operations: 14.3 us -> 0.71 us
  other arithmetic: 8 us -> 0.68 us
  matrix products: 5.09 us -> 0.13 us
    psum x1 -> x0, waiting for transfers between devices: 137 us -> none  [per_device(): whole = lax.psum(whole, 'tp')]
    psum x2 -> x0, blocking collectives: 93.1 us -> none  [the longest x1 68.9 us: per_device(): lax.psum(jnp.concatenate([jnp.sum(lat_f * lat_f, axis=1), jnp.sum(ctx_f *...]
    pallas_call x1, Pallas kernels: 90.5 us -> 118 us  [per_device(): pl.pallas_call(main_kernel, out_shape=jax.ShapeDtypeStruct((rows, 64), bf...]
    dot_general x3 -> x1, matrix products: 5.09 us -> 0.13 us  [nn(): return jnp.dot(lhs, rhs, preferred_element_type=jnp.float32)]
  transfers between devices with their start and end apart: 1 -> 0, of which waited for: 1 -> 0; matrix products, arithmetic and copies ran while one was open for 1% -> 0% of each run, Pallas kernels for 0% -> 0%
where the time goes in v2:
time: 124 us
  Pallas kernels  118 us (95%)
  local copies, waits for them, and re-layouts  4.76 us (4%)
    pallas_call x1, Pallas kernels, per_device(): pl.pallas_call(main_kernel, out_shape=jax.ShapeDtypeStruct((rows, 64), bf...  118 us
    unnamed x6, local copies, waits for them, and re-layouts  2.48 us

profile of v2, /device:TPU:1, one launch (start us, length us, event | category | flops | bytes accessed | tf_op | source)
XLA Modules:
  0.0 123.9 jit_solution(1064416763447279173)
XLA Ops:
  0.0 0.0 copy-start
  0.0 0.0 copy-start.1
  0.7 0.1 copy-done
  0.8 0.7 convert_bitcast_fusion
  1.5 0.1 fusion
  1.6 0.7 reshape.10.mod_ref
  2.3 1.5 %copy.21.latent_ref = bf16[384,64]{1,0:T(8,128)(2,1)} copy(bf16[384,64]{0,1:T(8,128)(2,1)} %param.19) | data formatting | bytes 98304 | tf_op args[0]
  3.9 0.0 copy-done.1
  3.9 0.8 copy.20
  4.7 117.7 %main.1 = bf16[384,64]{1,0:T(8,128)(2,1)} custom-call(bf16[384,64]{1,0:T(8,128)(2,1)} %copy.21.latent_ref, bf16[32,64]{1,0:T(8,128)(2,1)} %context_ref.1, f32[1,384]{1,0:T(1,128)} %reshape.10.mod_ref, f32[1,64]{1,0:T(1,128)} %bitcast.20, bf16[64,512]{1,0:T(8,128)(2,1)} %w_dq_ref.1, bf16[64,512]{1,0:T(8,128)(2,1)} %w_dkv_ref.1, bf16[64,64]{1,0:T(8,128)(2,1)} %w_kr_ref.1, ...), custom_call_target="tpu_custom_call" | custom-call | tf_op jit(solution)/shard_map/main/pallas_call | solution.py:638
  122.3 1.6 %copy.22 = bf16[384,64]{0,1:T(8,128)(2,1)} copy(bf16[384,64]{1,0:T(8,128)(2,1)} %main.1) | data formatting | bytes 98304 | tf_op jit(solution)/shard_map/main/pallas_call | solution.py:638
Async XLA Ops:
  0.0 0.8 copy-start
  0.0 3.8 %copy-start.1 = (bf16[512,1,192]{0,2,1:T(8,128)(2,1)S(1)}, bf16[512,1,192]{0,2,1:T(8,128)(2,1)}, u32[]{:S(2)}) copy-start(bf16[512,1,192]{0,2,1:T(8,128)(2,1)} %param.30) | copy-start | bytes 589828

commit v3 on v2

--- a/solution.py
+++ b/solution.py
@@ -84,125 +84,165 @@
 
 
 class PlaneGather:
-    def __init__(self, at, buf, owners, part, sems):
-        s1, r1, s2, r2, sd, rd = sems
+    def __init__(self, at, buf, owners, way, sems):
         self.at = at
         self.buf = buf
         self.owners = owners
-        self.part = part
-        self.s1, self.r1, self.s2, self.r2, self.sd, self.rd = s1, r1, s2, r2, sd, rd
+        self.way = way
+        self.s1, self.r1, self.s2, self.r2, self.sd, self.rd = sems
         self.offsets = (0, -1, 1, 2)
+        self.a, self.b = (at.a, at.b) if way == 0 else (at.b, at.a)
+
+    def natural(self, a, b):
+        return (a, b) if self.way == 0 else (b, a)
+
+    def dev(self, a, b):
+        return self.at.dev(*self.natural(a, b))
 
     def exists(self, a, b):
+        a, b = self.natural(a, b)
         return 4 * a + b < self.owners
 
-    def slot(self, k, a, b):
-        return self.buf.at[k, self.at.c * 16 + 4 * a + b]
+    def block(self, k, a, b, core=None):
+        a, b = self.natural(a, b)
+        core = self.at.c if core is None else core
+        return self.buf.at[k, core * 16 + 4 * a + b, pl.ds(2 * self.way, 2)]
 
     def half(self, k, a, b, h):
-        return self.buf.at[k, self.at.c * 16 + 4 * a + b, pl.ds(self.part * h, self.part)]
+        a, b = self.natural(a, b)
+        return self.buf.at[k, self.at.c * 16 + 4 * a + b, pl.ds(2 * self.way + h, 1)]
+
+    def across(self, k, a, b, j, m):
+        block = self.block(k, a, b)
+        send(block, block, self.sd.at[k, self.way, j, m], self.rd.at[k, self.way, j, m], self.at.partner())
 
     def first_start(self, k):
-        at = self.at
-
-        @pl.when(self.exists(at.a, at.b))
-        def _():
-            own = self.slot(k, at.a, at.b)
-            send(own, own, self.s1.at[k, 0], self.r1.at[k, 0], at.dev(around(at.a, 1), at.b))
-            send(own, own, self.s1.at[k, 1], self.r1.at[k, 1], at.dev(around(at.a, -1), at.b))
+        @pl.when(self.exists(self.a, self.b))
+        def _():
+            own = self.block(k, self.a, self.b)
+            for role, by in ((0, 1), (1, -1)):
+                send(own, own, self.s1.at[k, self.way, role], self.r1.at[k, self.way, role], self.dev(around(self.a, by), self.b))
 
     def first_forward(self, k):
-        at = self.at
         for role, by in ((0, -1), (1, 1)):
-            a = around(at.a, by)
-
-            @pl.when(self.exists(a, at.b))
+            a = around(self.a, by)
+
+            @pl.when(self.exists(a, self.b))
             def _():
-                arrived(self.slot(k, a, at.b), self.r1.at[k, role])
-                part = self.half(k, a, at.b, role)
-                send(part, part, self.s1.at[k, 2 + role], self.r1.at[k, 2 + role], at.dev(around(at.a, -by), at.b))
+                arrived(self.block(k, a, self.b), self.r1.at[k, self.way, role])
+                part = self.half(k, a, self.b, role)
+                send(
+                    part,
+                    part,
+                    self.s1.at[k, self.way, 2 + role],
+                    self.r1.at[k, self.way, 2 + role],
+                    self.dev(around(self.a, -by), self.b),
+                )
 
     def first_end(self, k):
-        at = self.at
-        a = around(at.a, 2)
-
-        @pl.when(self.exists(a, at.b))
+        a = around(self.a, 2)
+
+        @pl.when(self.exists(a, self.b))
         def _():
             for role in (0, 1):
-                arrived(self.half(k, a, at.b, role), self.r1.at[k, 2 + role])
+                arrived(self.half(k, a, self.b, role), self.r1.at[k, self.way, 2 + role])
 
     def second_start(self, k, j):
-        at = self.at
-        a = around(at.a, self.offsets[j])
-
-        @pl.when(self.exists(a, at.b))
-        def _():
-            own = self.slot(k, a, at.b)
-            send(own, own, self.s2.at[k, j, 0], self.r2.at[k, j, 0], at.dev(at.a, around(at.b, 1)))
-            send(own, own, self.s2.at[k, j, 1], self.r2.at[k, j, 1], at.dev(at.a, around(at.b, -1)))
+        a = around(self.a, self.offsets[j])
+
+        @pl.when(self.exists(a, self.b))
+        def _():
+            own = self.block(k, a, self.b)
+            for role, by in ((0, 1), (1, -1)):
+                send(
+                    own, own, self.s2.at[k, self.way, j, role], self.r2.at[k, self.way, j, role], self.dev(self.a, around(self.b, by))
+                )
+            self.across(k, a, self.b, j, 0)
 
     def second_forward(self, k, j):
-        at = self.at
-        a = around(at.a, self.offsets[j])
+        a = around(self.a, self.offsets[j])
         for role, by in ((0, -1), (1, 1)):
-            b = around(at.b, by)
+            b = around(self.b, by)
 
             @pl.when(self.exists(a, b))
             def _():
-                arrived(self.slot(k, a, b), self.r2.at[k, j, role])
+                arrived(self.block(k, a, b), self.r2.at[k, self.way, j, role])
                 part = self.half(k, a, b, role)
-                send(part, part, self.s2.at[k, j, 2 + role], self.r2.at[k, j, 2 + role], at.dev(at.a, around(at.b, -by)))
+                send(
+                    part,
+                    part,
+                    self.s2.at[k, self.way, j, 2 + role],
+                    self.r2.at[k, self.way, j, 2 + role],
+                    self.dev(self.a, around(self.b, -by)),
+                )
+                self.across(k, a, b, j, 1 + role)
 
     def second_end(self, k, j):
-        at = self.at
-        a = around(at.a, self.offsets[j])
-        b = around(at.b, 2)
+        a = around(self.a, self.offsets[j])
+        b = around(self.b, 2)
 
         @pl.when(self.exists(a, b))
         def _():
             for role in (0, 1):
-                arrived(self.half(k, a, b, role), self.r2.at[k, j, 2 + role])
-
-        row = self.buf.at[k, pl.ds(at.c * 16 + 4 * a, 4)]
-        send(row, row, self.sd.at[k, j], self.rd.at[k, j], at.partner())
+                arrived(self.half(k, a, b, role), self.r2.at[k, self.way, j, 2 + role])
+            self.across(k, a, b, j, 3)
 
     def other_core(self, k):
-        at = self.at
         for j in range(4):
-            a = around(at.b, self.offsets[j])
-            arrived(self.buf.at[k, pl.ds((1 - at.c) * 16 + 4 * a, 4)], self.rd.at[k, j])
+            a = around(self.b, self.offsets[j])
+            for m in range(4):
+                b = around(self.a, self.offsets[m])
+
+                @pl.when(self.exists(a, b))
+                def _():
+                    arrived(self.block(k, a, b, 1 - self.at.c), self.rd.at[k, self.way, j, m])
 
     def all_sent(self, k):
-        at = self.at
-        own = self.slot(k, 0, 0)
+        own = self.block(k, 0, 0)
         part = self.half(k, 0, 0, 0)
 
-        @pl.when(self.exists(at.a, at.b))
-        def _():
-            arrived(own, self.s1.at[k, 0])
-            arrived(own, self.s1.at[k, 1])
+        @pl.when(self.exists(self.a, self.b))
+        def _():
+            arrived(own, self.s1.at[k, self.way, 0])
+            arrived(own, self.s1.at[k, self.way, 1])
 
         for role, by in ((0, -1), (1, 1)):
 
-            @pl.when(self.exists(around(at.a, by), at.b))
+            @pl.when(self.exists(around(self.a, by), self.b))
             def _():
-                arrived(part, self.s1.at[k, 2 + role])
+                arrived(part, self.s1.at[k, self.way, 2 + role])
 
         for j in range(4):
-            a = around(at.a, self.offsets[j])
-
-            @pl.when(self.exists(a, at.b))
+            a = around(self.a, self.offsets[j])
+
+            @pl.when(self.exists(a, self.b))
             def _():
-                arrived(own, self.s2.at[k, j, 0])
-                arrived(own, self.s2.at[k, j, 1])
+                arrived(own, self.s2.at[k, self.way, j, 0])
+                arrived(own, self.s2.at[k, self.way, j, 1])
+                arrived(own, self.sd.at[k, self.way, j, 0])
 
             for role, by in ((0, -1), (1, 1)):
 
-                @pl.when(self.exists(a, around(at.b, by)))
+                @pl.when(self.exists(a, around(self.b, by)))
                 def _():
-                    arrived(part, self.s2.at[k, j, 2 + role])
-
-            arrived(self.buf.at[k, pl.ds(0, 4)], self.sd.at[k, j])
+                    arrived(part, self.s2.at[k, self.way, j, 2 + role])
+                    arrived(own, self.sd.at[k, self.way, j, 1 + role])
+
+            @pl.when(self.exists(a, around(self.b, 2)))
+            def _():
+                arrived(own, self.sd.at[k, self.way, j, 3])
+
+
+class BothWays:
+    def __init__(self, at, buf, owners, sems):
+        self.ways = [PlaneGather(at, buf, owners, way, sems) for way in range(2)]
+
+    def __getattr__(self, name):
+        def call(*args):
+            for way in self.ways:
+                getattr(way, name)(*args)
+
+        return call
 
 
 def swapped(values):
@@ -218,7 +258,9 @@
 def main_kernel(
     latent_ref,
     context_ref,
-    mod_ref,
+    cond_ref,
+    cond_ctx_ref,
+    w_mod_ref,
     g_norm_ref,
     w_dq_ref,
     w_dkv_ref,
@@ -234,6 +276,8 @@
     w_ukv_hbm,
     w_out_hbm,
     out_ref,
+    latent,
+    mod_part,
     mod_in,
     mod_mine,
     mod_all,
@@ -297,14 +341,19 @@
     for load in loads:
         load.start()
 
-    half_rows = w_dq_ref.shape[0] // 2
-    for h in range(2):
-        rows = pl.ds(h * half_rows, half_rows)
-        w_down[0, own_slot, h, :, 0:512] = w_dq_ref[rows, :]
-        w_down[0, own_slot, h, :, 512:1024] = w_dkv_ref[rows, :]
-        w_down[0, own_slot, h, :, 1024:1152] = jnp.concatenate(
-            [w_kr_ref[rows, :], jnp.zeros((half_rows, 64), jnp.bfloat16)], axis=1
+    for n in range(4):
+        rows = pl.ds(n * 16, 16)
+        w_down[0, own_slot, n, :, 0:512] = w_dq_ref[rows, :]
+        w_down[0, own_slot, n, :, 512:1024] = w_dkv_ref[rows, :]
+        w_down[0, own_slot, n, :, 1024:1152] = jnp.concatenate(
+            [w_kr_ref[rows, :], jnp.zeros((16, 64), jnp.bfloat16)], axis=1
         )
+    latent[...] = jnp.transpose(latent_ref[...].astype(jnp.float32)).astype(jnp.bfloat16)
+    signal = jnp.concatenate([cond_ref[...], cond_ctx_ref[...], jnp.zeros((6, 128), jnp.bfloat16)], axis=0)
+    signal = jax.nn.silu(signal.astype(jnp.float32)).astype(jnp.bfloat16)
+    partial_mod = nt(signal, w_mod_ref[...])
+    mod_part[:, 0:192] = partial_mod[0:1]
+    mod_part[:, 192:384] = partial_mod[1:2]
     mod_mine[...] = jnp.zeros(mod_mine.shape, jnp.float32)
     peak[...] = jnp.full(peak.shape, -1e30, jnp.float32)
     total[...] = jnp.zeros(total.shape, jnp.float32)
@@ -313,9 +362,9 @@
     pl.semaphore_wait(barrier, 46)
 
     for n in range(1, SP):
-        send(mod_ref, mod_in.at[n - 1], ms, mr, (lax.rem(at.z - REL[n] + SP, SP), at.t))
-
-    down = PlaneGather(at, w_down, 16, 1, down_sems)
+        send(mod_part, mod_in.at[n - 1], ms, mr, (lax.rem(at.z - REL[n] + SP, SP), at.t))
+
+    down = BothWays(at, w_down, 16, down_sems)
     down.first_start(0)
     down.second_start(0, 0)
 
@@ -334,7 +383,7 @@
             x_all[own_slot] = source[...]
 
     def give_latent(i, carry):
-        give(i, latent_ref.at[pl.ds(pl.multiple_of(i * BLOCK, BLOCK), BLOCK)])
+        give(i, latent.at[pl.ds(pl.multiple_of(i * BLOCK, BLOCK), BLOCK)])
         return carry
 
     lax.fori_loop(0, 24, give_latent, 0)
@@ -353,7 +402,7 @@
     down.second_forward(0, 0)
 
     arrived(mod_in, mr)
-    mod = mod_ref[...]
+    mod = mod_part[...]
     for n in range(SP - 1):
         mod = mod + mod_in[n]
     mod_mine[:, 0:384] = mod
@@ -401,8 +450,8 @@
     item[:, 0:512] = low_norm(low[:, 512:1024], g_ckv_ref[...])
     item[:, 512:640] = rotary.astype(jnp.bfloat16)
     cq = low_norm(low[:, 0:512], g_cq_ref[...])
-    compressed[0, own_slot, 0] = cq[:, 0:256]
-    compressed[0, own_slot, 1] = cq[:, 256:512]
+    for n in range(4):
+        compressed[0, own_slot, n] = cq[:, 128 * n : 128 * n + 128]
 
     @pl.when(owner)
     def _():
@@ -417,8 +466,8 @@
                 (lax.rem(at.z - REL[n] + SP, SP), at.t),
             )
 
-    ask = PlaneGather(at, compressed, OWNERS, 1, cq_sems)
-    gather = PlaneGather(at, keys, OWNERS, 2, key_sems)
+    ask = BothWays(at, compressed, OWNERS, cq_sems)
+    gather = BothWays(at, keys, OWNERS, key_sems)
     ask.first_start(0)
     ask.second_start(0, 0)
     ask.first_forward(0)
@@ -462,13 +511,15 @@
 
     def make_query():
         ask.other_core(0)
-        pieces = [compressed[0, pl.ds(16 * c, 13 - 2 * c), h] for c in range(2) for h in range(2)]
-        pieces = [piece.reshape(-1, 256) for piece in pieces]
         cq = jnp.concatenate(
-            [jnp.concatenate(pieces[0:2], axis=1), jnp.concatenate(pieces[2:4], axis=1)], axis=0
+            [
+                jnp.concatenate([compressed[0, pl.ds(16 * c, 13 - 2 * c), n].reshape(-1, 128) for n in range(4)], axis=1)
+                for c in range(2)
+            ],
+            axis=0,
         )
-        query[:, 0:NOPE] = nn(cq, w_uq[:, 0:NOPE]).astype(jnp.bfloat16)
-        turn = nn(cq, w_uq[:, NOPE:])
+        query[:, 0:NOPE] = nt(cq, w_uq[0:NOPE, :]).astype(jnp.bfloat16)
+        turn = nt(cq, w_uq[NOPE:, :])
         turn = jnp.concatenate([turn, jnp.zeros_like(turn)], axis=1)
         for r in range(6):
             values = turn[64 * r : 64 * r + 64]
@@ -555,14 +606,14 @@
     send(sums, sums_in, xs, xr, at.partner())
     gate = mod_mine[:, 128:192]
 
-    def finish(value, start):
-        value = jnp.where(at.c == 0, value[:, :64], value[:, 64:])
-        where = pl.ds(start, rows)
-        out_ref[where, :] = (latent_ref[where, :].astype(jnp.float32) + gate * value).astype(jnp.bfloat16)
-
-    finish(here, at.c * rows)
+    def columns_here(value):
+        return gate * jnp.where(at.c == 0, value[:, :64], value[:, 64:])
+
+    here = columns_here(here)
     arrived(sums_in, xr)
-    finish(sums_in[...], (1 - at.c) * rows)
+    there = columns_here(sums_in[...])
+    branch = jnp.concatenate([jnp.where(at.c == 0, here, there), jnp.where(at.c == 0, there, here)], axis=0)
+    out_ref[...] = (latent_ref[...].astype(jnp.float32) + jnp.transpose(branch)).astype(jnp.bfloat16)
 
     arrived(mod_in, ms)
     arrived(mod_all.at[pl.ds(0, 31)], vs)
@@ -594,14 +645,8 @@
 
 def gather_sems(chunks):
     dma = pltpu.SemaphoreType.DMA
-    return [
-        dma((chunks, 4)),
-        dma((chunks, 4)),
-        dma((chunks, 4, 4)),
-        dma((chunks, 4, 4)),
-        dma((chunks, 4)),
-        dma((chunks, 4)),
-    ]
+    few, many = dma((chunks, 2, 4)), dma((chunks, 2, 4, 4))
+    return [few, few, many, many, many, many]
 
 
 def turn_tables():
@@ -626,10 +671,6 @@
     latent, context, cond, cond_ctx, w_mod, g_norm, w_dq, w_dkv, w_kr, g_cq, g_ckv, w_uq, w_ukv, ctx_lift, w_out
 ):
     rows = latent.shape[0]
-    signal = jnp.stack(
-        [jax.nn.silu(cond.astype(jnp.float32)), jax.nn.silu(cond_ctx.astype(jnp.float32))]
-    ).astype(jnp.bfloat16)
-    partial_mod = nn(signal, w_mod.reshape(w_mod.shape[0], -1)).reshape(1, 384)
     vmem = pl.BlockSpec(memory_space=pltpu.VMEM)
     smem = pl.BlockSpec(memory_space=pltpu.SMEM)
     hbm = pl.BlockSpec(memory_space=pltpu.HBM)
@@ -637,19 +678,21 @@
     bf16, f32 = jnp.bfloat16, jnp.float32
     return pl.pallas_call(
         main_kernel,
-        out_shape=jax.ShapeDtypeStruct((rows, 64), bf16),
-        in_specs=[vmem] * 9 + [smem] + [vmem] * 4 + [hbm] * 3,
+        out_shape=jax.ShapeDtypeStruct((64, rows), bf16),
+        in_specs=[vmem] * 11 + [smem] + [vmem] * 4 + [hbm] * 3,
         out_specs=vmem,
         scratch_shapes=[
+            pltpu.VMEM((rows, 64), bf16),
+            pltpu.VMEM((1, 384), f32),
             pltpu.VMEM((SP - 1, 1, 384), f32),
             pltpu.VMEM((1, 512), f32),
             pltpu.VMEM((32, 1, 512), f32),
             pltpu.VMEM((32, BLOCK, 64), bf16),
             pltpu.VMEM((BLOCK, D), bf16),
-            pltpu.VMEM((1, 32, 2, 32, 1152), bf16),
-            pltpu.VMEM((1, 32, 2, BLOCK, 256), bf16),
+            pltpu.VMEM((1, 32, 4, 16, 1152), bf16),
+            pltpu.VMEM((1, 32, 4, BLOCK, 128), bf16),
             pltpu.VMEM((BLOCK, 640), bf16),
-            pltpu.VMEM((512, NOPE + ROPE), bf16),
+            pltpu.VMEM((NOPE + ROPE, 512), bf16),
             pltpu.VMEM((512, NOPE + DV), bf16),
             pltpu.VMEM((DV, 512), bf16),
             pltpu.VMEM((DV, D), bf16),
@@ -683,9 +726,11 @@
         ),
         name="main",
     )(
-        latent,
+        latent.T,
         context,
-        partial_mod,
+        cond[None, :],
+        cond_ctx[None, :],
+        jnp.transpose(w_mod, (1, 2, 0)).reshape(192, 128),
         g_norm[None, :],
         w_dq,
         w_dkv,
@@ -694,10 +739,10 @@
         g_ckv[None, :],
         ctx_lift.reshape(1, 1),
         *turn_tables(),
-        w_uq[:, 0, :],
+        w_uq[:, 0, :].T,
         w_ukv[:, 0, :],
         w_out[0],
-    )
+    ).T
 
 
 def solution(mesh):

time: 124 us -> 122 us (0.984)
  local copies, waits for them, and re-layouts: 4.76 us -> 1.42 us
  Pallas kernels: 118 us -> 120 us
    pallas_call x1, Pallas kernels: 118 us -> 120 us  [per_device(): pl.pallas_call(main_kernel, out_shape=jax.ShapeDtypeStruct((64, rows), bf...]
    pallas_call x1 -> x0, local copies, waits for them, and re-layouts: 1.6 us -> none  [per_device(): pl.pallas_call(main_kernel, out_shape=jax.ShapeDtypeStruct((rows, 64), bf...]
    unnamed x6 -> x1, local copies, waits for them, and re-layouts: 2.48 us -> 1.42 us
where the time goes in v3:
time: 122 us
  Pallas kernels  120 us (98%)
  local copies, waits for them, and re-layouts  1.42 us (1%)
    pallas_call x1, Pallas kernels, per_device(): pl.pallas_call(main_kernel, out_shape=jax.ShapeDtypeStruct((64, rows), bf...  120 us

profile of v3, /device:TPU:1, one launch (start us, length us, event | category | flops | bytes accessed | tf_op | source)
XLA Modules:
  0.0 122.1 jit_solution(5246046601318989692)
XLA Ops:
  0.7 120.1 %main.1 = bf16[64,384]{1,0:T(8,128)(2,1)} custom-call(bf16[64,384]{1,0:T(8,128)(2,1)} %bitcast.21, bf16[32,64]{1,0:T(8,128)(2,1)} %context_ref.1, bf16[1,128]{1,0:T(2,128)(2,1)} %bitcast.25, bf16[1,128]{1,0:T(2,128)(2,1)} %bitcast.26, bf16[192,128]{1,0:T(8,128)(2,1)} %bitcast.22, f32[1,64]{1,0:T(1,128)} %bitcast.27, bf16[64,512]{1,0:T(8,128)(2,1)} %w_dq_ref.1, ...), custom_call_target="tpu_custom_call" | custom-call | tf_op jit(solution)/shard_map/main/pallas_call | solution.py:679
  120.7 1.4 %copy.22 = bf16[384,64]{0,1:T(8,128)(2,1)} copy(bf16[384,64]{0,1:T(8,128)(2,1)} %bitcast.19) | data formatting | bytes 98304

commit v4 on v3

--- a/solution.py
+++ b/solution.py
@@ -393,13 +393,10 @@
     down.first_forward(0)
     down.second_start(0, 1)
     down.second_start(0, 2)
-    loads[2].wait()
-    send(w_out, w_other, ws, wr, at.partner())
     loads[1].wait()
     w_uvt[...] = jnp.transpose(w_up[:, NOPE:].astype(jnp.float32)).astype(jnp.bfloat16)
     down.first_end(0)
     down.second_start(0, 3)
-    down.second_forward(0, 0)
 
     arrived(mod_in, mr)
     mod = mod_part[...]
@@ -415,11 +412,8 @@
 
     lax.fori_loop(1, 32, tell, 0)
 
-    for j in (1, 2, 3):
+    for j in range(4):
         down.second_forward(0, j)
-    loads[0].wait()
-    for j in range(4):
-        down.second_end(0, j)
 
     @pl.when(owner)
     def _():
@@ -428,6 +422,10 @@
     x = x_all[...].astype(jnp.float32)
     squares = jnp.sum(jnp.sum(x * x, axis=0), axis=1, keepdims=True)
     norm = lax.rsqrt(squares / D + EPS)
+    for j in range(4):
+        down.second_end(0, j)
+    loads[2].wait()
+    send(w_out, w_other, ws, wr, at.partner())
     arrived(mod_all.at[pl.ds(0, 31)], vr)
     for s in range(0, 32, 2):
         pair = []
@@ -470,9 +468,6 @@
     gather = BothWays(at, keys, OWNERS, key_sems)
     ask.first_start(0)
     ask.second_start(0, 0)
-    ask.first_forward(0)
-    ask.second_start(0, 1)
-    ask.second_start(0, 2)
 
     def chunk_here(k):
         @pl.when(owner)
@@ -501,15 +496,26 @@
         arrived(keys.at[0, own_slot, pl.ds(1, 3)], zr.at[0])
 
     gather.first_start(0)
+    gather.second_start(0, 0)
+    ask.first_forward(0)
+    ask.second_start(0, 1)
+    ask.second_start(0, 2)
+    gather.first_forward(0)
+    gather.second_start(0, 1)
+    gather.second_start(0, 2)
     ask.first_end(0)
     ask.second_start(0, 3)
+    gather.first_end(0)
+    gather.second_start(0, 3)
+    chunk_here(1)
+    gather.first_start(1)
     for j in range(4):
         ask.second_forward(0, j)
-    gather.second_start(0, 0)
     for j in range(4):
         ask.second_end(0, j)
 
     def make_query():
+        loads[0].wait()
         ask.other_core(0)
         cq = jnp.concatenate(
             [
@@ -528,13 +534,10 @@
             query[64 * r : 64 * r + 64, NOPE:] = (values * cosine + swapped(values) * sine).astype(jnp.bfloat16)
 
     def step(k, carry):
-        last = k == CHUNKS
-
-        @pl.when(jnp.logical_not(last))
-        def _():
-            gather.first_forward(k)
-            gather.second_start(k, 1)
-            gather.second_start(k, 2)
+        @pl.when(k < CHUNKS)
+        def _():
+            gather.second_forward(k, 0)
+            gather.second_forward(k, 1)
 
         @pl.when(k == 0)
         def _():
@@ -544,38 +547,37 @@
         def _():
             attend(k - 1, at.c)
 
-        @pl.when(jnp.logical_not(last))
-        def _():
-            gather.first_end(k)
-            gather.second_start(k, 3)
-            gather.second_forward(k, 0)
-
         @pl.when(k < CHUNKS - 1)
         def _():
-            chunk_here(k + 1)
-            gather.first_start(k + 1)
+            gather.first_forward(k + 1)
+            gather.second_start(k + 1, 0)
+            gather.second_start(k + 1, 1)
+            gather.second_start(k + 1, 2)
+
+        @pl.when(k < CHUNKS)
+        def _():
+            gather.second_forward(k, 2)
+            gather.second_forward(k, 3)
+
+        @pl.when(k < CHUNKS - 1)
+        def _():
+            gather.first_end(k + 1)
+            gather.second_start(k + 1, 3)
+
+        @pl.when(k < CHUNKS - 2)
+        def _():
+            chunk_here(k + 2)
+            gather.first_start(k + 2)
 
         @pl.when(k > 0)
         def _():
             gather.other_core(k - 1)
             attend(k - 1, 1 - at.c)
 
-        @pl.when(jnp.logical_not(last))
-        def _():
-            gather.second_forward(k, 1)
-            gather.second_forward(k, 2)
-            gather.second_end(k, 0)
-            gather.second_forward(k, 3)
-
-        @pl.when(k < CHUNKS - 1)
-        def _():
-            gather.second_start(k + 1, 0)
-
-        @pl.when(jnp.logical_not(last))
-        def _():
-            gather.second_end(k, 1)
-            gather.second_end(k, 2)
-            gather.second_end(k, 3)
+        @pl.when(k < CHUNKS)
+        def _():
+            for j in range(4):
+                gather.second_end(k, j)
 
         return carry
 

time: 122 us -> 111 us (0.910)
  Pallas kernels: 120 us -> 108 us
    pallas_call x1, Pallas kernels: 120 us -> 108 us  [per_device(): pl.pallas_call(main_kernel, out_shape=jax.ShapeDtypeStruct((64, rows), bf...]
where the time goes in v4:
time: 111 us; the launch traced here: 110 us
  Pallas kernels  108 us (97%)
  local copies, waits for them, and re-layouts  1.42 us (1%)
    pallas_call x1, Pallas kernels, per_device(): pl.pallas_call(main_kernel, out_shape=jax.ShapeDtypeStruct((64, rows), bf...  108 us

profile of v4, /device:TPU:1, one launch (start us, length us, event | category | flops | bytes accessed | tf_op | source)
XLA Modules:
  0.0 110.3 jit_solution(16213643794655126467)
XLA Ops:
  0.7 108.2 %main.1 = bf16[64,384]{1,0:T(8,128)(2,1)} custom-call(bf16[64,384]{1,0:T(8,128)(2,1)} %bitcast.21, bf16[32,64]{1,0:T(8,128)(2,1)} %context_ref.1, bf16[1,128]{1,0:T(2,128)(2,1)} %bitcast.25, bf16[1,128]{1,0:T(2,128)(2,1)} %bitcast.26, bf16[192,128]{1,0:T(8,128)(2,1)} %bitcast.22, f32[1,64]{1,0:T(1,128)} %bitcast.27, bf16[64,512]{1,0:T(8,128)(2,1)} %w_dq_ref.1, ...), custom_call_target="tpu_custom_call" | custom-call | tf_op jit(solution)/shard_map/main/pallas_call | solution.py:681
  108.9 1.4 %copy.22 = bf16[384,64]{0,1:T(8,128)(2,1)} copy(bf16[384,64]{0,1:T(8,128)(2,1)} %bitcast.19) | data formatting | bytes 98304

commit v5 on v4

--- a/solution.py
+++ b/solution.py
@@ -85,6 +85,7 @@
 
 class PlaneGather:
     def __init__(self, at, buf, owners, way, sems):
+        self.size = buf.shape[2] // 2
         self.at = at
         self.buf = buf
         self.owners = owners
@@ -106,11 +107,7 @@
     def block(self, k, a, b, core=None):
         a, b = self.natural(a, b)
         core = self.at.c if core is None else core
-        return self.buf.at[k, core * 16 + 4 * a + b, pl.ds(2 * self.way, 2)]
-
-    def half(self, k, a, b, h):
-        a, b = self.natural(a, b)
-        return self.buf.at[k, self.at.c * 16 + 4 * a + b, pl.ds(2 * self.way + h, 1)]
+        return self.buf.at[k, core * 16 + 4 * a + b, pl.ds(self.size * self.way, self.size)]
 
     def across(self, k, a, b, j, m):
         block = self.block(k, a, b)
@@ -129,23 +126,17 @@
 
             @pl.when(self.exists(a, self.b))
             def _():
-                arrived(self.block(k, a, self.b), self.r1.at[k, self.way, role])
-                part = self.half(k, a, self.b, role)
-                send(
-                    part,
-                    part,
-                    self.s1.at[k, self.way, 2 + role],
-                    self.r1.at[k, self.way, 2 + role],
-                    self.dev(around(self.a, -by), self.b),
-                )
+                block = self.block(k, a, self.b)
+                arrived(block, self.r1.at[k, self.way, role])
+                if role == self.way:
+                    send(block, block, self.s1.at[k, self.way, 2], self.r1.at[k, self.way, 2], self.dev(around(self.a, -by), self.b))
 
     def first_end(self, k):
         a = around(self.a, 2)
 
         @pl.when(self.exists(a, self.b))
         def _():
-            for role in (0, 1):
-                arrived(self.half(k, a, self.b, role), self.r1.at[k, self.way, 2 + role])
+            arrived(self.block(k, a, self.b), self.r1.at[k, self.way, 2])
 
     def second_start(self, k, j):
         a = around(self.a, self.offsets[j])
@@ -166,15 +157,16 @@
 
             @pl.when(self.exists(a, b))
             def _():
-                arrived(self.block(k, a, b), self.r2.at[k, self.way, j, role])
-                part = self.half(k, a, b, role)
-                send(
-                    part,
-                    part,
-                    self.s2.at[k, self.way, j, 2 + role],
-                    self.r2.at[k, self.way, j, 2 + role],
-                    self.dev(self.a, around(self.b, -by)),
-                )
+                block = self.block(k, a, b)
+                arrived(block, self.r2.at[k, self.way, j, role])
+                if role == j % 2:
+                    send(
+                        block,
+                        block,
+                        self.s2.at[k, self.way, j, 2],
+                        self.r2.at[k, self.way, j, 2],
+                        self.dev(self.a, around(self.b, -by)),
+                    )
                 self.across(k, a, b, j, 1 + role)
 
     def second_end(self, k, j):
@@ -183,8 +175,7 @@
 
         @pl.when(self.exists(a, b))
         def _():
-            for role in (0, 1):
-                arrived(self.half(k, a, b, role), self.r2.at[k, self.way, j, 2 + role])
+            arrived(self.block(k, a, b), self.r2.at[k, self.way, j, 2])
             self.across(k, a, b, j, 3)
 
     def other_core(self, k):
@@ -199,18 +190,15 @@
 
     def all_sent(self, k):
         own = self.block(k, 0, 0)
-        part = self.half(k, 0, 0, 0)
 
         @pl.when(self.exists(self.a, self.b))
         def _():
             arrived(own, self.s1.at[k, self.way, 0])
             arrived(own, self.s1.at[k, self.way, 1])
 
-        for role, by in ((0, -1), (1, 1)):
-
-            @pl.when(self.exists(around(self.a, by), self.b))
-            def _():
-                arrived(part, self.s1.at[k, self.way, 2 + role])
+        @pl.when(self.exists(around(self.a, 1 if self.way else -1), self.b))
+        def _():
+            arrived(own, self.s1.at[k, self.way, 2])
 
         for j in range(4):
             a = around(self.a, self.offsets[j])
@@ -225,7 +213,8 @@
 
                 @pl.when(self.exists(a, around(self.b, by)))
                 def _():
-                    arrived(part, self.s2.at[k, self.way, j, 2 + role])
+                    if role == j % 2:
+                        arrived(own, self.s2.at[k, self.way, j, 2])
                     arrived(own, self.sd.at[k, self.way, j, 1 + role])
 
             @pl.when(self.exists(a, around(self.b, 2)))
@@ -286,6 +275,8 @@
     w_down,
     compressed,
     item,
+    turned,
+    turned_in,
     w_uq,
     w_up,
     w_uvt,
@@ -310,6 +301,8 @@
     vr,
     zs,
     zr,
+    ts,
+    tr,
     *rest,
 ):
     down_sems, cq_sems, key_sems = rest[0:6], rest[6:12], rest[12:18]
@@ -445,45 +438,68 @@
     item_sin = jnp.where(in_context, 0.0, row_sin_ref[pl.ds(item_row, 1), :] + col_sin_ref[item_col, :])
     rotary = low[:, 1024:1152]
     rotary = rotary * item_cos + swapped(rotary) * item_sin
-    item[:, 0:512] = low_norm(low[:, 512:1024], g_ckv_ref[...])
-    item[:, 512:640] = rotary.astype(jnp.bfloat16)
+    ckv_own = low_norm(low[:, 512:1024], g_ckv_ref[...])
+    for n in range(4):
+        item[n] = ckv_own[:, 128 * n : 128 * n + 128]
+    turned[...] = (rotary + pltpu.roll(rotary, 64, 1)).astype(jnp.bfloat16)
     cq = low_norm(low[:, 0:512], g_cq_ref[...])
     for n in range(4):
         compressed[0, own_slot, n] = cq[:, 128 * n : 128 * n + 128]
 
     @pl.when(owner)
     def _():
-        keys[0, own_slot, 0] = item[...]
+        keys[0, own_slot, 0:4] = item[...]
+        turned_in[0, 0] = turned[...]
         for n in range(1, SP):
             k, i = divmod(n, 4)
-            send(
-                item,
-                keys.at[k, own_slot, i],
-                zs.at[k],
-                zr.at[k],
-                (lax.rem(at.z - REL[n] + SP, SP), at.t),
-            )
+            there = (lax.rem(at.z - REL[n] + SP, SP), at.t)
+            send(item, keys.at[k, own_slot, pl.ds(9 * (i // 2) + 4 * (i % 2), 4)], zs.at[k], zr.at[k], there)
+            send(turned, turned_in.at[k, i], ts.at[k], tr.at[k], there)
 
     ask = BothWays(at, compressed, OWNERS, cq_sems)
     gather = BothWays(at, keys, OWNERS, key_sems)
     ask.first_start(0)
     ask.second_start(0, 0)
 
+    def join_turned(k):
+        for way in range(2):
+            first = turned_in[k, 2 * way].astype(jnp.float32)
+            second = turned_in[k, 2 * way + 1].astype(jnp.float32)
+            lane = lax.broadcasted_iota(jnp.int32, first.shape, 1)
+            keys[k, own_slot, 9 * way + 8] = jnp.where(lane < 64, first, second).astype(jnp.bfloat16)
+
     def chunk_here(k):
         @pl.when(owner)
         def _():
-            arrived(keys.at[k, own_slot], zr.at[k])
+            arrived(keys.at[k, own_slot, pl.ds(0, 16)], zr.at[k])
+            arrived(turned_in.at[k], tr.at[k])
+            join_turned(k)
 
     lift = lift_ref[0, 0] * LOG2E
 
     def attend(k, g):
-        block = keys[k, pl.ds(g * 16, OWNERS)].reshape(OWNERS * 4 * BLOCK, 640)
-        ckv = block[:, :512]
-        key = jnp.concatenate([nn(ckv, w_up[:, :NOPE]).astype(jnp.bfloat16), block[:, 512:]], axis=1)
+        slots = pl.ds(g * 16, OWNERS)
+        count = OWNERS * BLOCK
+        ckv = jnp.concatenate(
+            [
+                jnp.concatenate([keys[k, slots, 9 * w + 4 * i + n].reshape(count, 128) for n in range(4)], axis=1)
+                for w in range(2)
+                for i in range(2)
+            ],
+            axis=0,
+        )
+        key = nn(ckv, w_up[:, :NOPE]).astype(jnp.bfloat16)
         value = nt(w_uvt[...], ckv).astype(jnp.bfloat16)
-        score = nt(key, query[...]) * (SCALE * LOG2E)
         extra = jnp.where(g == 1, lift, 0.0)
-        score = jnp.concatenate([score[: 11 * 4 * BLOCK], score[11 * 4 * BLOCK :] + extra], axis=0)
+        scores = []
+        for w in range(2):
+            rotary_key = keys[k, slots, 9 * w + 8].reshape(count, 128)
+            for i in range(2):
+                first = (2 * w + i) * count
+                both = jnp.concatenate([key[first : first + count], rotary_key], axis=1)
+                part = nt(both, query[i]) * (SCALE * LOG2E)
+                scores += [part[: 11 * BLOCK], part[11 * BLOCK :] + extra]
+        score = jnp.concatenate(scores, axis=0)
         fresh = jnp.maximum(peak[...], jnp.max(score, axis=0, keepdims=True))
         probs = jnp.exp2(score - fresh)
         fade = jnp.exp2(peak[...] - fresh)
@@ -493,7 +509,9 @@
 
     @pl.when(owner)
     def _():
-        arrived(keys.at[0, own_slot, pl.ds(1, 3)], zr.at[0])
+        arrived(keys.at[0, own_slot, pl.ds(0, 12)], zr.at[0])
+        arrived(turned_in.at[0, pl.ds(1, 3)], tr.at[0])
+        join_turned(0)
 
     gather.first_start(0)
     gather.second_start(0, 0)
@@ -524,14 +542,18 @@
             ],
             axis=0,
         )
-        query[:, 0:NOPE] = nt(cq, w_uq[0:NOPE, :]).astype(jnp.bfloat16)
+        plain = nt(cq, w_uq[0:NOPE, :]).astype(jnp.bfloat16)
+        query[0, :, 0:NOPE] = plain
+        query[1, :, 0:NOPE] = plain
         turn = nt(cq, w_uq[NOPE:, :])
         turn = jnp.concatenate([turn, jnp.zeros_like(turn)], axis=1)
         for r in range(6):
             values = turn[64 * r : 64 * r + 64]
             cosine = row_cos_ref[pl.ds(first_row + r, 1), :] + col_cos_ref[...]
             sine = row_sin_ref[pl.ds(first_row + r, 1), :] + col_sin_ref[...]
-            query[64 * r : 64 * r + 64, NOPE:] = (values * cosine + swapped(values) * sine).astype(jnp.bfloat16)
+            values = values * cosine + swapped(values) * sine
+            query[0, 64 * r : 64 * r + 64, NOPE:] = values.astype(jnp.bfloat16)
+            query[1, 64 * r : 64 * r + 64, NOPE:] = pltpu.roll(values, 64, 1).astype(jnp.bfloat16)
 
     def step(k, carry):
         @pl.when(k < CHUNKS)
@@ -601,7 +623,35 @@
         pieces[n] = product(p).astype(jnp.bfloat16)
         send(pieces.at[n], pieces_in.at[n], ps, pr, (at.z, 2 * p + at.c))
     here = product(at.p)
+    arrived(mod_in, ms)
+    arrived(mod_all.at[pl.ds(0, 31)], vs)
+    arrived(w_other, ws)
+    arrived(heads_in, hs)
+
+    @pl.when(owner)
+    def _():
+        arrived(x_all.at[pl.ds(0, 25)], as_)
+        arrived(keys.at[0, 0, pl.ds(0, 12)], zs.at[0])
+        arrived(turned_in.at[0, pl.ds(1, 3)], ts.at[0])
+        for k in range(1, CHUNKS):
+            arrived(keys.at[k, 0, pl.ds(0, 16)], zs.at[k])
+            arrived(turned_in.at[k], ts.at[k])
+
+    @pl.when(jnp.logical_not(owner))
+    def _():
+        arrived(x_all.at[pl.ds(0, 26)], as_)
+
+    down.all_sent(0)
+    ask.all_sent(0)
+
+    def sent(k, carry):
+        gather.all_sent(k)
+        return carry
+
+    lax.fori_loop(0, CHUNKS, sent, 0)
+
     arrived(pieces_in, pr)
+    arrived(pieces_in, ps)
     for n in range(15):
         here = here + pieces_in[n].astype(jnp.float32)
     sums[...] = here
@@ -616,33 +666,7 @@
     there = columns_here(sums_in[...])
     branch = jnp.concatenate([jnp.where(at.c == 0, here, there), jnp.where(at.c == 0, there, here)], axis=0)
     out_ref[...] = (latent_ref[...].astype(jnp.float32) + jnp.transpose(branch)).astype(jnp.bfloat16)
-
-    arrived(mod_in, ms)
-    arrived(mod_all.at[pl.ds(0, 31)], vs)
-    arrived(w_other, ws)
-    arrived(heads_in, hs)
-    arrived(pieces_in, ps)
     arrived(sums_in, xs)
-
-    @pl.when(owner)
-    def _():
-        arrived(x_all.at[pl.ds(0, 25)], as_)
-        arrived(keys.at[0, 0, pl.ds(1, 3)], zs.at[0])
-        for k in range(1, CHUNKS):
-            arrived(keys.at[k, 0], zs.at[k])
-
-    @pl.when(jnp.logical_not(owner))
-    def _():
-        arrived(x_all.at[pl.ds(0, 26)], as_)
-
-    down.all_sent(0)
-    ask.all_sent(0)
-
-    def sent(k, carry):
-        gather.all_sent(k)
-        return carry
-
-    lax.fori_loop(0, CHUNKS, sent, 0)
 
 
 def gather_sems(chunks):
@@ -693,13 +717,15 @@
             pltpu.VMEM((BLOCK, D), bf16),
             pltpu.VMEM((1, 32, 4, 16, 1152), bf16),
             pltpu.VMEM((1, 32, 4, BLOCK, 128), bf16),
-            pltpu.VMEM((BLOCK, 640), bf16),
+            pltpu.VMEM((4, BLOCK, 128), bf16),
+            pltpu.VMEM((BLOCK, 128), bf16),
+            pltpu.VMEM((CHUNKS, 4, BLOCK, 128), bf16),
             pltpu.VMEM((NOPE + ROPE, 512), bf16),
             pltpu.VMEM((512, NOPE + DV), bf16),
             pltpu.VMEM((DV, 512), bf16),
             pltpu.VMEM((DV, D), bf16),
-            pltpu.VMEM((rows, 256), bf16),
-            pltpu.VMEM((CHUNKS, 32, 4, BLOCK, 640), bf16),
+            pltpu.VMEM((2, rows, 256), bf16),
+            pltpu.VMEM((CHUNKS, 32, 18, BLOCK, 128), bf16),
             pltpu.VMEM((1, rows), f32),
             pltpu.VMEM((1, rows), f32),
             pltpu.VMEM((DV, rows), f32),
@@ -716,6 +742,8 @@
             dma,
             dma,
             dma,
+            dma((CHUNKS,)),
+            dma((CHUNKS,)),
             dma((CHUNKS,)),
             dma((CHUNKS,)),
             *gather_sems(1),

time: 111 us -> 109 us (0.982)
    pallas_call x1, Pallas kernels: 108 us -> 107 us  [per_device(): pl.pallas_call(main_kernel, out_shape=jax.ShapeDtypeStruct((64, rows), bf...]
where the time goes in v5:
time: 109 us
  Pallas kernels  107 us (98%)
  local copies, waits for them, and re-layouts  1.42 us (1%)
    pallas_call x1, Pallas kernels, per_device(): pl.pallas_call(main_kernel, out_shape=jax.ShapeDtypeStruct((64, rows), bf...  107 us

profile of v5, /device:TPU:1, one launch (start us, length us, event | category | flops | bytes accessed | tf_op | source)
XLA Modules:
  0.0 108.7 jit_solution(168061057967615977)
XLA Ops:
  0.7 106.6 %main.1 = bf16[64,384]{1,0:T(8,128)(2,1)} custom-call(bf16[64,384]{1,0:T(8,128)(2,1)} %bitcast.21, bf16[32,64]{1,0:T(8,128)(2,1)} %context_ref.1, bf16[1,128]{1,0:T(2,128)(2,1)} %bitcast.25, bf16[1,128]{1,0:T(2,128)(2,1)} %bitcast.26, bf16[192,128]{1,0:T(8,128)(2,1)} %bitcast.22, f32[1,64]{1,0:T(1,128)} %bitcast.27, bf16[64,512]{1,0:T(8,128)(2,1)} %w_dq_ref.1, ...), custom_call_target="tpu_custom_call" | custom-call | tf_op jit(solution)/shard_map/main/pallas_call | solution.py:705
  107.2 1.4 %copy.22 = bf16[384,64]{0,1:T(8,128)(2,1)} copy(bf16[384,64]{0,1:T(8,128)(2,1)} %bitcast.19) | data formatting | bytes 98304

commit v6 on v5

--- a/solution.py
+++ b/solution.py
@@ -361,28 +361,6 @@
     down.first_start(0)
     down.second_start(0, 0)
 
-    def give(i, source):
-        c = lax.div(i, OWNERS)
-        l = i - c * OWNERS
-        a, b = lax.div(l, 4), lax.rem(l, 4)
-        t = 2 * ((4 * b + a) * (1 - c) + (4 * a + b) * c) + c
-
-        @pl.when(t != at.t)
-        def _():
-            send(source, x_all.at[own_slot], as_, ar, (at.z, t))
-
-        @pl.when(t == at.t)
-        def _():
-            x_all[own_slot] = source[...]
-
-    def give_latent(i, carry):
-        give(i, latent.at[pl.ds(pl.multiple_of(i * BLOCK, BLOCK), BLOCK)])
-        return carry
-
-    lax.fori_loop(0, 24, give_latent, 0)
-    for i in (24, 25):
-        give(jnp.int32(i), context_ref.at[pl.ds((i - 24) * BLOCK, BLOCK)])
-
     down.first_forward(0)
     down.second_start(0, 1)
     down.second_start(0, 2)
@@ -390,6 +368,29 @@
     w_uvt[...] = jnp.transpose(w_up[:, NOPE:].astype(jnp.float32)).astype(jnp.bfloat16)
     down.first_end(0)
     down.second_start(0, 3)
+
+    def give(i, source):
+        c = lax.div(i, OWNERS)
+        l = i - c * OWNERS
+        a, b = lax.div(l, 4), lax.rem(l, 4)
+        t = 2 * ((4 * b + a) * (1 - c) + (4 * a + b) * c) + c
+
+        @pl.when(t != at.t)
+        def _():
+            send(source, x_all.at[own_slot], as_, ar, (at.z, t))
+
+        @pl.when(t == at.t)
+        def _():
+            x_all[own_slot] = source[...]
+
+    def give_latent(i, carry):
+        give(i, latent.at[pl.ds(pl.multiple_of(i * BLOCK, BLOCK), BLOCK)])
+        return carry
+
+    lax.fori_loop(0, 24, give_latent, 0)
+    for i in (24, 25):
+        give(jnp.int32(i), context_ref.at[pl.ds((i - 24) * BLOCK, BLOCK)])
+
 
     arrived(mod_in, mr)
     mod = mod_part[...]
@@ -609,18 +610,23 @@
     heads[...] = jnp.transpose(accum[...] / total[...]).astype(jnp.bfloat16)
     theirs = heads.at[pl.ds((1 - at.c) * rows, rows)]
     send(theirs, heads_in, hs, hr, at.partner())
+    mine = heads[pl.ds(at.c * rows, rows), :]
+
+    def columns_of(p):
+        return pl.ds(pl.multiple_of(p * 128, 128), 128)
+
+    targets = [4 * around(at.y, dy) + around(at.x, dx) for dy, dx in FAR_FIRST]
+    early = [nn(mine, w_out[:, columns_of(p)]) for p in targets[:6]]
     arrived(w_other, wr)
     arrived(heads_in, hr)
-    mine = heads[pl.ds(at.c * rows, rows), :]
     other = heads_in[...]
 
-    def product(p):
-        columns = pl.ds(pl.multiple_of(p * 128, 128), 128)
-        return nn(mine, w_out[:, columns]) + nn(other, w_other[:, columns])
-
-    for n, (dy, dx) in enumerate(FAR_FIRST):
-        p = 4 * around(at.y, dy) + around(at.x, dx)
-        pieces[n] = product(p).astype(jnp.bfloat16)
+    def product(p, own=None):
+        own = nn(mine, w_out[:, columns_of(p)]) if own is None else own
+        return own + nn(other, w_other[:, columns_of(p)])
+
+    for n, p in enumerate(targets):
+        pieces[n] = product(p, early[n] if n < len(early) else None).astype(jnp.bfloat16)
         send(pieces.at[n], pieces_in.at[n], ps, pr, (at.z, 2 * p + at.c))
     here = product(at.p)
     arrived(mod_in, ms)

time: 109 us -> 109 us (level)
  no operation moved by 1% of the time
where the time goes in v6:
time: 109 us; the launch traced here: 108 us
  Pallas kernels  106 us (97%)
  local copies, waits for them, and re-layouts  1.42 us (1%)
    pallas_call x1, Pallas kernels, per_device(): pl.pallas_call(main_kernel, out_shape=jax.ShapeDtypeStruct((64, rows), bf...  106 us

profile of v6, /device:TPU:1, one launch (start us, length us, event | category | flops | bytes accessed | tf_op | source)
XLA Modules:
  0.0 108.4 jit_solution(6362599090900638471)
XLA Ops:
  0.7 106.4 %main.1 = bf16[64,384]{1,0:T(8,128)(2,1)} custom-call(bf16[64,384]{1,0:T(8,128)(2,1)} %bitcast.21, bf16[32,64]{1,0:T(8,128)(2,1)} %context_ref.1, bf16[1,128]{1,0:T(2,128)(2,1)} %bitcast.25, bf16[1,128]{1,0:T(2,128)(2,1)} %bitcast.26, bf16[192,128]{1,0:T(8,128)(2,1)} %bitcast.22, f32[1,64]{1,0:T(1,128)} %bitcast.27, bf16[64,512]{1,0:T(8,128)(2,1)} %w_dq_ref.1, ...), custom_call_target="tpu_custom_call" | custom-call | tf_op jit(solution)/shard_map/main/pallas_call | solution.py:711
  107.0 1.4 %copy.22 = bf16[384,64]{0,1:T(8,128)(2,1)} copy(bf16[384,64]{0,1:T(8,128)(2,1)} %bitcast.19) | data formatting | bytes 98304
